TPU v7x, 128 devices: a whole 4x4x4 slice. The times are simulated.
128 devices in a mesh: fs: 16 (over z, x), tp: 8 (over y, core).
Axes of the slice: x: 4, y: 4, z: 4, core: 2. Of those that a mesh axis runs over, the one named last changes fastest.
Arguments:
- resid: bfloat16 [16384, 2048], P(('fs', 'tp')), may hold values from -6 to 6
- mix_gain: float32 [2048], replicated, may hold values from 0.1 to 1.9
- in_weight: bfloat16 [2048, 2048], P('fs', 'tp'), may hold values from -0.125 to 0.125
- conv_taps: float32 [4, 2048], P(None, 'tp'), may hold values from -3 to 3
- recur_gate_w: bfloat16 [32, 64, 64], P('tp'), may hold values from -0.75 to 0.75
- input_gate_w: bfloat16 [32, 64, 64], P('tp'), may hold values from -0.75 to 0.75
- decay_rate: float32 [2048], P('tp'), may hold values from 0.0004 to 0.03
- out_weight: bfloat16 [2048, 2048], P('tp', 'fs'), may hold values from -0.25 to 0.25
- mlp_gain: float32 [2048], replicated, may hold values from 0.1 to 1.9
- up_gate_w: bfloat16 [2048, 5632], P('fs', 'tp'), may hold values from -0.125 to 0.125
- up_val_w: bfloat16 [2048, 5632], P('fs', 'tp'), may hold values from -0.125 to 0.125
- ffn_taps: float32 [3, 5632], P(None, 'tp'), may hold values from -3 to 3
- down_weight: bfloat16 [5632, 2048], P('tp', 'fs'), may hold values from -0.15625 to 0.15625
Outputs:
- result: bfloat16 [16384, 2048], P(('fs', 'tp'))
All inputs are finite; a program needn't handle non-finite values.
Results may differ from a plain program's by a relative error of at most 0.028.
Values may be sent and summed in bfloat16 or wider, within the bound.
No kernel may reach another device: no remote copies, remote signals or barrier semaphores. Data moves between devices by JAX's collectives and lax.ppermute only.
A program may use at most 64 MiB of HBM per device.

v0:
```python
import jax
import jax.numpy as jnp
from jax import lax
from jax.experimental import pallas as pl
from jax.experimental.pallas import tpu as pltpu
from jax.sharding import Mesh
from jax.sharding import PartitionSpec as P


SEQ = 128
D = 2048
BLK = 128
HID = 704
F32 = jnp.float32
BF16 = jnp.bfloat16
MIB = 1024 * 1024
FS = ("z", "x")
TP = ("y", "c")
FS_TP = ("z", "x", "y", "c")


def fetch(a, axis, ahead):
    size = lax.axis_size(axis)
    return lax.ppermute(a, axis, [(i, (i - ahead) % size) for i in range(size)])


def fetch_all(a, axis):
    return [a] + [fetch(a, axis, k) for k in (1, 2, 3)]


def partner(a):
    return fetch(a, "c", 1)


VM = pl.BlockSpec(memory_space=pltpu.VMEM)
SM = pl.BlockSpec(memory_space=pltpu.SMEM)


def call(body, out, *args, vmem=4, scalars=0, flops=0, scratch=()):
    return pl.pallas_call(
        body,
        in_specs=[SM] * scalars + [VM] * (len(args) - scalars),
        out_shape=out,
        scratch_shapes=[pltpu.VMEM(*v) for v in scratch],
        compiler_params=pltpu.CompilerParams(vmem_limit_bytes=vmem * MIB),
        cost_estimate=pl.CostEstimate(
            flops=flops, transcendentals=0, bytes_accessed=0
        ),
    )(*args)


def sds(shape, dtype=BF16):
    return jax.ShapeDtypeStruct(shape, dtype)


def first_body(order, resid, gain, gain2, in_w, out_w, resid_rel, normed_rel, gain2_rel, a, b):
    wide = resid[...].astype(F32)
    scale = lax.rsqrt(jnp.mean(wide * wide, axis=-1, keepdims=True) + 1e-06)
    for j in range(D // BLK):
        at = pl.multiple_of(order[j] * BLK, BLK)
        block = resid[:, pl.ds(at, BLK)]
        put = slice(j * BLK, (j + 1) * BLK)
        resid_rel[:, put] = block
        normed_rel[:, put] = (block.astype(F32) * scale * gain[:, pl.ds(at, BLK)]).astype(BF16)
        gain2_rel[:, put] = gain2[:, pl.ds(at, BLK)]
    for half, dst in enumerate((a, b)):
        dst[:BLK] = in_w[:, half * BLK : (half + 1) * BLK]
        dst[BLK:] = out_w[half * BLK : (half + 1) * BLK]


def halves_body(gate, val, down, a, b):
    a[:HID] = gate[...]
    a[HID:] = down[: HID // 2]
    b[:HID] = val[...]
    b[HID:] = down[HID // 2 :]


def second_norm_body(resid, p0, p1, p2, p3, gain, middle, normed):
    total = (p0[...].astype(F32) + p1[...].astype(F32)) + (p2[...].astype(F32) + p3[...].astype(F32))
    mid = (resid[...].astype(F32) + total).astype(BF16)
    middle[...] = mid
    wide = mid.astype(F32)
    scale = lax.rsqrt(jnp.mean(wide * wide, axis=-1, keepdims=True) + 1e-06)
    normed[...] = (wide * scale * gain[...]).astype(BF16)


def last_sum_body(order, middle, p0, p1, p2, p3, out):
    for j in range(D // BLK):
        at = pl.multiple_of(order[j] * BLK, BLK)
        put = slice(j * BLK, (j + 1) * BLK)
        total = (p0[:, put].astype(F32) + p1[:, put].astype(F32)) + (
            p2[:, put].astype(F32) + p3[:, put].astype(F32)
        )
        out[:, pl.ds(at, BLK)] = (middle[:, put].astype(F32) + total).astype(BF16)


def delayed(v, steps, rows, fill):
    return jnp.where(rows >= steps, pltpu.roll(v, steps, 0), fill)


def sigmoid(v):
    return 1.0 / (1.0 + jnp.exp(-v))


def minus_expm1(v, exp_v):
    series = jnp.full_like(v, 1.0 / 9.0)
    series = 1.0 + v * series
    for k in (8.0, 7.0, 6.0, 5.0, 4.0, 3.0, 2.0):
        series = 1.0 + v * series * (1.0 / k)
    return jnp.where(v > -0.5, -v * series, 1.0 - exp_v)


def mix_body(x, in_own, in_par, taps, gates, rate, out_own, out_par, out, proj, states):
    rows = lax.broadcasted_iota(jnp.int32, (SEQ, BLK), 0)
    for half, w in enumerate((in_own, in_par)):
        proj[:, half * 256 : (half + 1) * 256] = jnp.dot(
            x[...], w[...], preferred_element_type=F32
        ).astype(BF16)

    def tile(t, carry):
        cols = pl.ds(pl.multiple_of(t * BLK, BLK), BLK)
        p = proj[:, cols].astype(F32)
        conv = p * taps[3:4, cols]
        for k in range(3):
            conv = conv + delayed(p, 3 - k, rows, 0.0) * taps[k : k + 1, cols]
        g = jnp.dot(conv.astype(BF16), gates[t], preferred_element_type=F32)
        rgate = sigmoid(g[:, :BLK])
        igate = sigmoid(g[:, BLK:])
        logdecay = -8.0 * rgate * rate[:, cols]
        a = jnp.exp(logdecay)
        b = jnp.sqrt(minus_expm1(2.0 * logdecay, a * a)) * (igate * conv)
        step = 1
        while step < SEQ:
            b = a * delayed(b, step, rows, 0.0) + b
            if step * 2 < SEQ:
                a = a * delayed(a, step, rows, 1.0)
            step *= 2
        states[:, cols] = b.astype(BF16)
        return carry

    lax.fori_loop(0, 4, tile, 0)

    def column(n, carry):
        cols = pl.ds(pl.multiple_of(n * 512, 512), 512)
        part = jnp.dot(states[:, :256], out_own[:, cols], preferred_element_type=F32)
        part = part + jnp.dot(states[:, 256:], out_par[:, cols], preferred_element_type=F32)
        out[:, cols] = part.astype(BF16)
        return carry

    lax.fori_loop(0, 4, column, 0)


def nt_dot(a, b):
    return lax.dot_general(a, b, (((1,), (1,)), ((), ())), preferred_element_type=F32)


def up_body(x, gate, val, taps, out):
    rows = lax.broadcasted_iota(jnp.int32, (SEQ, BLK), 0)

    def tile(t, carry):
        cols = pl.ds(pl.multiple_of(t * BLK, BLK), BLK)
        both = nt_dot(x[...], jnp.concatenate([gate[cols], val[cols]], axis=0))
        both = both.astype(BF16).astype(F32)
        g, v = both[:, :BLK], both[:, BLK:]
        conv = g * taps[2:3, cols]
        for k in range(2):
            conv = conv + delayed(g, 2 - k, rows, 0.0) * taps[k : k + 1, cols]
        out[:, cols] = (conv * sigmoid(conv) * v).astype(BF16)
        return carry

    lax.fori_loop(0, 2 * HID // BLK, tile, 0)


def down_body(h, down, out):
    def tile(n, carry):
        cols = pl.ds(pl.multiple_of(n * 512, 512), 512)
        out[:, cols] = jnp.dot(h[...], down[:, cols], preferred_element_type=F32).astype(BF16)
        return carry

    lax.fori_loop(0, 4, tile, 0)


def sums_sent(part, ahead):
    return fetch(part, "y", (-ahead) % 4)


def in_lanes(pieces):
    return jnp.concatenate(pieces, axis=1)


def layer(
    resid,
    mix_gain,
    in_weight,
    conv_taps,
    recur_gate_w,
    input_gate_w,
    decay_rate,
    out_weight,
    mlp_gain,
    up_gate_w,
    up_val_w,
    ffn_taps,
    down_weight,
):
    z, x = lax.axis_index("z"), lax.axis_index("x")
    steps = jnp.arange(16, dtype=jnp.int32)
    order = ((steps // 4 + z) % 4) * 4 + (steps % 4 + x) % 4

    resid_rel, normed, gain2, a, b = call(
        first_body,
        [sds((SEQ, D)), sds((SEQ, D)), sds((1, D), F32), sds((256, BLK)), sds((256, BLK))],
        order,
        resid,
        mix_gain.reshape(1, D),
        mlp_gain.reshape(1, D),
        in_weight,
        out_weight,
        scalars=1,
    )
    rows1 = fetch_all(normed, "y")

    a = jnp.stack(fetch_all(a, "x"))
    b = jnp.stack(fetch_all(b, "z"))
    a = fetch_all(a, "z")
    b = fetch_all(b, "x")
    a = [a[i][j] for i in range(4) for j in range(4)]
    b = [b[j][i] for i in range(4) for j in range(4)]
    in_own = jnp.concatenate(
        [jnp.concatenate([v[:BLK] for v in h], axis=0) for h in (a, b)], axis=1
    )
    out_own = jnp.concatenate([in_lanes([v[BLK:] for v in h]) for h in (a, b)], axis=0)
    in_par, out_par = partner(in_own), partner(out_own)

    gates = jnp.stack([recur_gate_w, input_gate_w])
    gates = jnp.concatenate([gates, partner(gates)], axis=1).reshape(2, 4, 2, 64, 64)
    zero = jnp.zeros_like(gates[:, :, 0])
    gates = jnp.concatenate(
        [
            jnp.concatenate([gates[:, :, 0], zero], axis=3),
            jnp.concatenate([zero, gates[:, :, 1]], axis=3),
        ],
        axis=2,
    )
    gates = jnp.concatenate([gates[0], gates[1]], axis=2)
    small = jnp.concatenate([conv_taps, decay_rate[None]], axis=0)
    small = jnp.concatenate([small, partner(small)], axis=1)
    taps, rate = small[:4], small[4:]
    ftaps = jnp.concatenate([ffn_taps, partner(ffn_taps)], axis=1)

    a, b = call(
        halves_body, [sds((1056, BLK)), sds((1056, BLK))], up_gate_w.T, up_val_w.T, down_weight
    )
    a = fetch_all(a, "x")
    b = fetch_all(b, "z")
    gate = in_lanes(fetch_all(in_lanes([v[:HID] for v in a]), "z"))
    val = fetch_all(jnp.stack([v[:HID] for v in b]), "x")
    val = in_lanes([val[j][i] for i in range(4) for j in range(4)])
    down_a = in_lanes(fetch_all(in_lanes([v[HID:] for v in a]), "z"))
    down_b = fetch_all(jnp.stack([v[HID:] for v in b]), "x")
    down_b = in_lanes([down_b[j][i] for i in range(4) for j in range(4)])
    down = jnp.concatenate([down_a, down_b], axis=0)
    gate = jnp.concatenate([gate, partner(gate)], axis=0)
    val = jnp.concatenate([val, partner(val)], axis=0)
    down = jnp.concatenate([down, partner(down)], axis=0)

    parts = [None] * 4
    for j in (1, 3, 2, 0):
        part = call(
            mix_body,
            sds((SEQ, D)),
            rows1[j],
            in_own,
            in_par,
            taps,
            gates,
            rate,
            out_own,
            out_par,
            flops=2 * SEQ * D * 512 * 2,
            scratch=[((SEQ, 512), BF16), ((SEQ, 512), BF16)],
        )
        parts[j] = sums_sent(part, j) if j else part
    middle, normed_two = call(
        second_norm_body, [sds((SEQ, D)), sds((SEQ, D))], resid_rel, *parts, gain2
    )
    rows2 = fetch_all(normed_two, "y")
    for j in (0, 1, 3, 2):
        hidden = call(
            up_body, sds((SEQ, 2 * HID)), rows2[j], gate, val, ftaps, flops=2 * SEQ * D * 1408 * 2
        )
        part = call(down_body, sds((SEQ, D)), hidden, down, flops=2 * SEQ * D * 1408)
        parts[j] = sums_sent(part, j) if j else part
    return call(last_sum_body, sds((SEQ, D)), order, middle, *parts, scalars=1)


def solution(mesh):
    split = Mesh(mesh.devices.reshape(4, 4, 4, 2), FS_TP)
    return jax.shard_map(
        layer,
        mesh=split,
        in_specs=(
            P(FS_TP, None),
            P(),
            P(FS, TP),
            P(None, TP),
            P(TP, None, None),
            P(TP, None, None),
            P(TP),
            P(TP, FS),
            P(),
            P(FS, TP),
            P(FS, TP),
            P(None, TP),
            P(TP, FS),
        ),
        out_specs=P(FS_TP, None),
        check_vma=False,
    )
```

profile of v0, /device:TPU:32, one launch (start us, length us, event | category | flops | bytes accessed | tf_op | source)
XLA Modules:
  0.0 280.6 jit_solution(18330996517444032647)
XLA Ops:
  21.4 4.6 %collective-permute-done.1 = bf16[256,128]{1,0:T(8,128)(2,1)S(1)} collective-permute-done((bf16[256,128]{1,0:T(8,128)(2,1)S(1)}, bf16[256,128]{1,0:T(8,128)(2,1)S(1)}, u32[]{:S(2)}, u32[]{:S(2)}) %collective-permute-start.1) | collective-permute-done | bytes 65568 | tf_op jit(solution)/shard_map/ppermute | solution.py:24
  29.6 3.1 %collective-permute-start.30 = (bf16[1056,128]{1,0:T(8,128)(2,1)S(1)}, bf16[1056,128]{1,0:T(8,128)(2,1)S(1)}, u32[]{:S(2)}, u32[]{:S(2)}) collective-permute-start(bf16[1056,128]{1,0:T(8,128)(2,1)S(1)} %get-tuple-element.22), channel_id=1, source_target_pairs={{0,64},{32,96},{64,0},{96,32},{1,65},{33,97},{65,1},{97,33},{2,66}... | collective-permute-start | bytes 811016 | tf_op jit(solution)/shard_map/ppermute | solution.py:24
  32.7 3.5 %collective-permute-done.22 = bf16[1056,128]{1,0:T(8,128)(2,1)S(1)} collective-permute-done((bf16[1056,128]{1,0:T(8,128)(2,1)S(1)}, bf16[1056,128]{1,0:T(8,128)(2,1)S(1)}, u32[]{:S(2)}, u32[]{:S(2)}) %collective-permute-start.22) | collective-permute-done | bytes 270368 | tf_op jit(solution)/shard_map/ppermute | solution.py:24
  41.1 2.9 %collective-permute-start.10 = (bf16[4,256,128]{2,1,0:T(8,128)(2,1)S(1)}, bf16[4,256,128]{2,1,0:T(8,128)(2,1)S(1)}, u32[]{:S(2)}, u32[]{:S(2)}) collective-permute-start(bf16[4,256,128]{2,1,0:T(8,128)(2,1)S(1)} %pad_maximum_fusion.11), channel_id=1, source_target_pairs={{0,16},{8,24},{16,0},{24,8},{1,17},{9,25},{17,1},{25,9},{2,18},{10... | collective-permute-start | bytes 786440 | tf_op jit(solution)/shard_map/ppermute | solution.py:24
  44.1 5.1 %collective-permute-start.3 = (bf16[4,256,128]{2,1,0:T(8,128)(2,1)S(1)}, bf16[4,256,128]{2,1,0:T(8,128)(2,1)S(1)}, u32[]{:S(2)}, u32[]{:S(2)}) collective-permute-start(bf16[4,256,128]{2,1,0:T(8,128)(2,1)S(1)} %pad_maximum_fusion.10), channel_id=1, source_target_pairs={{0,96},{32,0},{64,32},{96,64},{1,97},{33,1},{65,33},{97,65},{2,98}... | collective-permute-start | bytes 786440 | tf_op jit(solution)/shard_map/ppermute | solution.py:24
  51.5 6.7 %collective-permute-start.25 = (bf16[704,512]{1,0:T(8,128)(2,1)S(1)}, bf16[704,512]{1,0:T(8,128)(2,1)S(1)}, u32[]{:S(2)}, u32[]{:S(2)}) collective-permute-start(bf16[704,512]{1,0:T(8,128)(2,1)S(1)} %pad_maximum_fusion.6), channel_id=1, source_target_pairs={{0,96},{32,0},{64,32},{96,64},{1,97},{33,1},{65,33},{97,65},{2,98}... | collective-permute-start | bytes 2162696 | tf_op jit(solution)/shard_map/ppermute | solution.py:24
  59.8 3.8 %collective-permute-start.40 = (bf16[4,352,128]{2,1,0:T(8,128)(2,1)S(1)}, bf16[4,352,128]{2,1,0:T(8,128)(2,1)S(1)}, u32[]{:S(2)}, u32[]{:S(2)}) collective-permute-start(bf16[4,352,128]{2,1,0:T(8,128)(2,1)S(1)} %pad_maximum_fusion.9), channel_id=1, source_target_pairs={{0,24},{8,0},{16,8},{24,16},{1,25},{9,1},{17,9},{25,17},{2,26},{10... | collective-permute-start | bytes 1081352 | tf_op jit(solution)/shard_map/ppermute | solution.py:24
  65.1 12.4 %collective-permute-done.40 = bf16[4,352,128]{2,1,0:T(8,128)(2,1)S(1)} collective-permute-done((bf16[4,352,128]{2,1,0:T(8,128)(2,1)S(1)}, bf16[4,352,128]{2,1,0:T(8,128)(2,1)S(1)}, u32[]{:S(2)}, u32[]{:S(2)}) %collective-permute-start.40) | collective-permute-done | bytes 360480 | tf_op jit(solution)/shard_map/ppermute | solution.py:24
  77.4 7.6 %collective-permute-start.37 = (bf16[352,512]{1,0:T(8,128)(2,1)S(1)}, bf16[352,512]{1,0:T(8,128)(2,1)S(1)}, u32[]{:S(2)}, u32[]{:S(2)}) collective-permute-start(bf16[352,512]{1,0:T(8,128)(2,1)S(1)} %pad_maximum_fusion.8), channel_id=1, source_target_pairs={{0,96},{32,0},{64,32},{96,64},{1,97},{33,1},{65,33},{97,65},{2,98}... | collective-permute-start | bytes 1081352 | tf_op jit(solution)/shard_map/ppermute | solution.py:24
  87.4 10.8 %collective-permute-done.37 = bf16[352,512]{1,0:T(8,128)(2,1)S(1)} collective-permute-done((bf16[352,512]{1,0:T(8,128)(2,1)S(1)}, bf16[352,512]{1,0:T(8,128)(2,1)S(1)}, u32[]{:S(2)}, u32[]{:S(2)}) %collective-permute-start.37) | collective-permute-done | bytes 360480 | tf_op jit(solution)/shard_map/ppermute | solution.py:24
  100.1 5.2 %collective-permute-done.38 = bf16[352,512]{1,0:T(8,128)(2,1)S(1)} collective-permute-done((bf16[352,512]{1,0:T(8,128)(2,1)S(1)}, bf16[352,512]{1,0:T(8,128)(2,1)S(1)}, u32[]{:S(2)}, u32[]{:S(2)}) %collective-permute-start.38) | collective-permute-done | bytes 360480 | tf_op jit(solution)/shard_map/ppermute | solution.py:24
  105.4 3.5 %collective-permute-start.32 = (bf16[4,704,128]{2,1,0:T(8,128)(2,1)S(1)}, bf16[4,704,128]{2,1,0:T(8,128)(2,1)S(1)}, u32[]{:S(2)}, u32[]{:S(2)}) collective-permute-start(bf16[4,704,128]{2,1,0:T(8,128)(2,1)S(1)} %pad_maximum_fusion.7), channel_id=1, source_target_pairs={{0,24},{8,0},{16,8},{24,16},{1,25},{9,1},{17,9},{25,17},{2,26},{10... | collective-permute-start | bytes 2162696 | tf_op jit(solution)/shard_map/ppermute | solution.py:24
  111.6 4.1 %collective-permute-done.27 = bf16[704,512]{1,0:T(8,128)(2,1)S(1)} collective-permute-done((bf16[704,512]{1,0:T(8,128)(2,1)S(1)}, bf16[704,512]{1,0:T(8,128)(2,1)S(1)}, u32[]{:S(2)}, u32[]{:S(2)}) %collective-permute-start.27) | collective-permute-done | bytes 720928 | tf_op jit(solution)/shard_map/ppermute | solution.py:24
  115.8 22.1 %collective-permute-done.32 = bf16[4,704,128]{2,1,0:T(8,128)(2,1)S(1)} collective-permute-done((bf16[4,704,128]{2,1,0:T(8,128)(2,1)S(1)}, bf16[4,704,128]{2,1,0:T(8,128)(2,1)S(1)}, u32[]{:S(2)}, u32[]{:S(2)}) %collective-permute-start.32) | collective-permute-done | bytes 720928 | tf_op jit(solution)/shard_map/ppermute | solution.py:24
  153.5 2.9 %shard_map.129 = bf16[128,2048]{1,0:T(8,128)(2,1)S(1)} custom-call(bf16[128,2048]{1,0:T(8,128)(2,1)S(1)} %collective-permute-done.16.x, bf16[2048,256]{1,0:T(8,128)(2,1)S(1)} %pad_maximum_fusion.4.in_own, bf16[2048,256]{1,0:T(8,128)(2,1)S(1)} %collective-permute-done.12.in_par, f32[4,512]{1,0:T(4,128)S(1)} %slice.734.taps, ...), custom_call_target="tpu_custom_call" | custom-call | flops 536870912 | tf_op jit(solution)/shard_map/pallas_call | solution.py:40
  156.4 10.4 %collective-permute-done.18.x = bf16[128,2048]{1,0:T(8,128)(2,1)S(1)} collective-permute-done((bf16[128,2048]{1,0:T(8,128)(2,1)S(1)}, bf16[128,2048]{1,0:T(8,128)(2,1)S(1)}, u32[]{:S(2)}, u32[]{:S(2)}) %collective-permute-start.18) | collective-permute-done | bytes 524320 | tf_op jit(solution)/shard_map/ppermute | solution.py:24
  167.9 2.9 %shard_map.130 = bf16[128,2048]{1,0:T(8,128)(2,1)S(1)} custom-call(bf16[128,2048]{1,0:T(8,128)(2,1)S(1)} %collective-permute-done.18.x, bf16[2048,256]{1,0:T(8,128)(2,1)S(1)} %pad_maximum_fusion.4.in_own, bf16[2048,256]{1,0:T(8,128)(2,1)S(1)} %collective-permute-done.12.in_par, f32[4,512]{1,0:T(4,128)S(1)} %slice.734.taps, ...), custom_call_target="tpu_custom_call" | custom-call | flops 536870912 | tf_op jit(solution)/shard_map/pallas_call | solution.py:40
  170.7 6.8 %collective-permute-done.20.x = bf16[128,2048]{1,0:T(8,128)(2,1)S(1)} collective-permute-done((bf16[128,2048]{1,0:T(8,128)(2,1)S(1)}, bf16[128,2048]{1,0:T(8,128)(2,1)S(1)}, u32[]{:S(2)}, u32[]{:S(2)}) %collective-permute-start.20) | collective-permute-done | bytes 524320 | tf_op jit(solution)/shard_map/ppermute | solution.py:24
  177.6 2.9 %shard_map.131 = bf16[128,2048]{1,0:T(8,128)(2,1)S(1)} custom-call(bf16[128,2048]{1,0:T(8,128)(2,1)S(1)} %collective-permute-done.20.x, bf16[2048,256]{1,0:T(8,128)(2,1)S(1)} %pad_maximum_fusion.4.in_own, bf16[2048,256]{1,0:T(8,128)(2,1)S(1)} %collective-permute-done.12.in_par, f32[4,512]{1,0:T(4,128)S(1)} %slice.734.taps, ...), custom_call_target="tpu_custom_call" | custom-call | flops 536870912 | tf_op jit(solution)/shard_map/pallas_call | solution.py:40
  180.8 8.4 %collective-permute-done.17.p1 = bf16[128,2048]{1,0:T(8,128)(2,1)S(1)} collective-permute-done((bf16[128,2048]{1,0:T(8,128)(2,1)S(1)}, bf16[128,2048]{1,0:T(8,128)(2,1)S(1)}, u32[]{:S(2)}, u32[]{:S(2)}) %collective-permute-start.17) | collective-permute-done | bytes 524320 | tf_op jit(solution)/shard_map/ppermute | solution.py:24
  192.8 7.3 %collective-permute-done.19.p2 = bf16[128,2048]{1,0:T(8,128)(2,1)S(1)} collective-permute-done((bf16[128,2048]{1,0:T(8,128)(2,1)S(1)}, bf16[128,2048]{1,0:T(8,128)(2,1)S(1)}, u32[]{:S(2)}, u32[]{:S(2)}) %collective-permute-start.19) | collective-permute-done | bytes 524320 | tf_op jit(solution)/shard_map/ppermute | solution.py:24
  200.0 6.0 %collective-permute-done.21.p3 = bf16[128,2048]{1,0:T(8,128)(2,1)S(1)} collective-permute-done((bf16[128,2048]{1,0:T(8,128)(2,1)S(1)}, bf16[128,2048]{1,0:T(8,128)(2,1)S(1)}, u32[]{:S(2)}, u32[]{:S(2)}) %collective-permute-start.21) | collective-permute-done | bytes 524320 | tf_op jit(solution)/shard_map/ppermute | solution.py:24
  210.8 7.0 %pad_maximum_fusion.2.down = bf16[1408,2048]{1,0:T(8,128)(2,1)S(1)} fusion(bf16[704,2048]{1,0:T(8,128)(2,1)} %collective-permute-done.43, bf16[352,2048]{1,0:T(8,128)(2,1)S(1)} %constant_dynamic-update-slice_fusion.94, bf16[352,2048]{1,0:T(8,128)(2,1)S(1)} %constant_dynamic-update-slice_fusion.87), kind=kLoop, calls=%fused_computation.2 | loop fusion | flops 17301504 | bytes 11534336 | tf_op jit(solution)/shard_map/concatenate | solution.py:265
  217.8 3.7 %pad_maximum_fusion.gate = bf16[1408,2048]{1,0:T(8,128)(2,1)S(1)} fusion(bf16[704,2048]{1,0:T(8,128)(2,1)} %collective-permute-done.28, bf16[704,2048]{1,0:T(8,128)(2,1)} %copy-done.11), kind=kLoop, calls=%fused_computation | loop fusion | flops 11534336 | bytes 11534336 | tf_op jit(solution)/shard_map/concatenate | solution.py:263
  221.5 6.2 %pad_maximum_fusion.1.val = bf16[1408,2048]{1,0:T(8,128)(2,1)} fusion(bf16[704,2048]{1,0:T(8,128)(2,1)} %collective-permute-done.35, bf16[704,2048]{1,0:T(8,128)(2,1)} %constant_dynamic-update-slice_fusion.71), kind=kLoop, calls=%fused_computation.1 | loop fusion | flops 11534336 | bytes 11534336 | tf_op jit(solution)/shard_map/concatenate | solution.py:264
  227.7 4.9 %collective-permute-done.44.x = bf16[128,2048]{1,0:T(8,128)(2,1)} collective-permute-done((bf16[128,2048]{1,0:T(8,128)(2,1)S(1)}, bf16[128,2048]{1,0:T(8,128)(2,1)}, u32[]{:S(2)}, u32[]{:S(2)}) %collective-permute-start.44) | collective-permute-done | bytes 524320 | tf_op jit(solution)/shard_map/ppermute | solution.py:24
  235.2 6.7 %shard_map.136.h = bf16[128,1408]{1,0:T(8,128)(2,1)S(1)} custom-call(bf16[128,2048]{1,0:T(8,128)(2,1)} %collective-permute-done.44.x, bf16[1408,2048]{1,0:T(8,128)(2,1)S(1)} %pad_maximum_fusion.gate, bf16[1408,2048]{1,0:T(8,128)(2,1)S(1)} %copy-done, f32[3,1408]{1,0:T(4,128)S(1)} %pad_maximum_fusion.15.taps), custom_call_target="tpu_custom_call" | custom-call | flops 1476395008 | tf_op jit(solution)/shard_map/pallas_call | solution.py:40
  243.6 6.7 %shard_map.138.h = bf16[128,1408]{1,0:T(8,128)(2,1)S(1)} custom-call(bf16[128,2048]{1,0:T(8,128)(2,1)} %collective-permute-done.46.x, bf16[1408,2048]{1,0:T(8,128)(2,1)S(1)} %pad_maximum_fusion.gate, bf16[1408,2048]{1,0:T(8,128)(2,1)S(1)} %copy-done, f32[3,1408]{1,0:T(4,128)S(1)} %pad_maximum_fusion.15.taps), custom_call_target="tpu_custom_call" | custom-call | flops 1476395008 | tf_op jit(solution)/shard_map/pallas_call | solution.py:40
  251.9 5.3 %collective-permute-start.47 = (bf16[128,2048]{1,0:T(8,128)(2,1)S(1)}, bf16[128,2048]{1,0:T(8,128)(2,1)S(1)}, u32[]{:S(2)}, u32[]{:S(2)}) collective-permute-start(bf16[128,2048]{1,0:T(8,128)(2,1)S(1)} %shard_map.139), channel_id=1, source_target_pairs={{0,4},{2,6},{4,0},{6,2},{1,5},{3,7},{5,1},{7,3},{8,12},{10,14},{12... | collective-permute-start | bytes 1572872 | tf_op jit(solution)/shard_map/ppermute | solution.py:24
  257.2 5.6 %shard_map.140.h = bf16[128,1408]{1,0:T(8,128)(2,1)S(1)} custom-call(bf16[128,2048]{1,0:T(8,128)(2,1)S(1)} %collective-permute-done.48.x, bf16[1408,2048]{1,0:T(8,128)(2,1)S(1)} %pad_maximum_fusion.gate, bf16[1408,2048]{1,0:T(8,128)(2,1)S(1)} %copy-done, f32[3,1408]{1,0:T(4,128)S(1)} %pad_maximum_fusion.15.taps), custom_call_target="tpu_custom_call" | custom-call | flops 1476395008 | tf_op jit(solution)/shard_map/pallas_call | solution.py:40
  264.6 5.7 %shard_map.134.h = bf16[128,1408]{1,0:T(8,128)(2,1)S(1)} custom-call(bf16[128,2048]{1,0:T(8,128)(2,1)S(1)} %get-tuple-element.20.x, bf16[1408,2048]{1,0:T(8,128)(2,1)S(1)} %pad_maximum_fusion.gate, bf16[1408,2048]{1,0:T(8,128)(2,1)S(1)} %bitcast.333, f32[3,1408]{1,0:T(4,128)S(1)} %pad_maximum_fusion.15.taps), custom_call_target="tpu_custom_call" | custom-call | flops 1476395008 | tf_op jit(solution)/shard_map/pallas_call | solution.py:40
  271.8 7.0 %collective-permute-done.49.p3 = bf16[128,2048]{1,0:T(8,128)(2,1)S(1)} collective-permute-done((bf16[128,2048]{1,0:T(8,128)(2,1)S(1)}, bf16[128,2048]{1,0:T(8,128)(2,1)S(1)}, u32[]{:S(2)}, u32[]{:S(2)}) %collective-permute-start.49) | collective-permute-done | bytes 524320 | tf_op jit(solution)/shard_map/ppermute | solution.py:24
  (228 shorter events, 77.9 us)
Async XLA Ops:
  5.1 24.3 %collective-permute-start.8 = (bf16[256,128]{1,0:T(8,128)(2,1)S(1)}, bf16[256,128]{1,0:T(8,128)(2,1)S(1)}, u32[]{:S(2)}, u32[]{:S(2)}) collective-permute-start(bf16[256,128]{1,0:T(8,128)(2,1)S(1)} %get-tuple-element.17), channel_id=1, source_target_pairs={{0,32},{32,64},{64,96},{96,0},{1,33},{33,65},{65,97},{97,1},{2,34}... | collective-permute-start | bytes 196616 | tf_op jit(solution)/shard_map/ppermute | solution.py:24
  7.1 22.4 %collective-permute-start.7 = (bf16[256,128]{1,0:T(8,128)(2,1)S(1)}, bf16[256,128]{1,0:T(8,128)(2,1)S(1)}, u32[]{:S(2)}, u32[]{:S(2)}) collective-permute-start(bf16[256,128]{1,0:T(8,128)(2,1)S(1)} %get-tuple-element.17), channel_id=1, source_target_pairs={{0,64},{32,96},{64,0},{96,32},{1,65},{33,97},{65,1},{97,33},{2,66}... | collective-permute-start | bytes 196616 | tf_op jit(solution)/shard_map/ppermute | solution.py:24
  8.2 21.4 %collective-permute-start.6 = (bf16[256,128]{1,0:T(8,128)(2,1)S(1)}, bf16[256,128]{1,0:T(8,128)(2,1)S(1)}, u32[]{:S(2)}, u32[]{:S(2)}) collective-permute-start(bf16[256,128]{1,0:T(8,128)(2,1)S(1)} %get-tuple-element.17), channel_id=1, source_target_pairs={{0,96},{32,0},{64,32},{96,64},{1,97},{33,1},{65,33},{97,65},{2,98}... | collective-permute-start | bytes 196616 | tf_op jit(solution)/shard_map/ppermute | solution.py:24
  26.0 18.1 %collective-permute-start.24 = (bf16[1056,128]{1,0:T(8,128)(2,1)S(1)}, bf16[1056,128]{1,0:T(8,128)(2,1)S(1)}, u32[]{:S(2)}, u32[]{:S(2)}) collective-permute-start(bf16[1056,128]{1,0:T(8,128)(2,1)S(1)} %get-tuple-element.21), channel_id=1, source_target_pairs={{0,8},{8,16},{16,24},{24,0},{1,9},{9,17},{17,25},{25,1},{2,10},{10... | collective-permute-start | bytes 811016 | tf_op jit(solution)/shard_map/ppermute | solution.py:24
  44.1 15.6 %collective-permute-start.3 = (bf16[4,256,128]{2,1,0:T(8,128)(2,1)S(1)}, bf16[4,256,128]{2,1,0:T(8,128)(2,1)S(1)}, u32[]{:S(2)}, u32[]{:S(2)}) collective-permute-start(bf16[4,256,128]{2,1,0:T(8,128)(2,1)S(1)} %pad_maximum_fusion.10), channel_id=1, source_target_pairs={{0,96},{32,0},{64,32},{96,64},{1,97},{33,1},{65,33},{97,65},{2,98}... | collective-permute-start | bytes 786440 | tf_op jit(solution)/shard_map/ppermute | solution.py:24
  51.5 58.0 %collective-permute-start.25 = (bf16[704,512]{1,0:T(8,128)(2,1)S(1)}, bf16[704,512]{1,0:T(8,128)(2,1)S(1)}, u32[]{:S(2)}, u32[]{:S(2)}) collective-permute-start(bf16[704,512]{1,0:T(8,128)(2,1)S(1)} %pad_maximum_fusion.6), channel_id=1, source_target_pairs={{0,96},{32,0},{64,32},{96,64},{1,97},{33,1},{65,33},{97,65},{2,98}... | collective-permute-start | bytes 2162696 | tf_op jit(solution)/shard_map/ppermute | solution.py:24
  58.2 53.2 %collective-permute-start.26 = (bf16[704,512]{1,0:T(8,128)(2,1)S(1)}, bf16[704,512]{1,0:T(8,128)(2,1)S(1)}, u32[]{:S(2)}, u32[]{:S(2)}) collective-permute-start(bf16[704,512]{1,0:T(8,128)(2,1)S(1)} %pad_maximum_fusion.6), channel_id=1, source_target_pairs={{0,64},{32,96},{64,0},{96,32},{1,65},{33,97},{65,1},{97,33},{2,66}... | collective-permute-start | bytes 2162696 | tf_op jit(solution)/shard_map/ppermute | solution.py:24
  59.8 17.7 %collective-permute-start.40 = (bf16[4,352,128]{2,1,0:T(8,128)(2,1)S(1)}, bf16[4,352,128]{2,1,0:T(8,128)(2,1)S(1)}, u32[]{:S(2)}, u32[]{:S(2)}) collective-permute-start(bf16[4,352,128]{2,1,0:T(8,128)(2,1)S(1)} %pad_maximum_fusion.9), channel_id=1, source_target_pairs={{0,24},{8,0},{16,8},{24,16},{1,25},{9,1},{17,9},{25,17},{2,26},{10... | collective-permute-start | bytes 1081352 | tf_op jit(solution)/shard_map/ppermute | solution.py:24
  63.6 21.5 %collective-permute-start.41 = (bf16[4,352,128]{2,1,0:T(8,128)(2,1)S(1)}, bf16[4,352,128]{2,1,0:T(8,128)(2,1)S(1)}, u32[]{:S(2)}, u32[]{:S(2)}) collective-permute-start(bf16[4,352,128]{2,1,0:T(8,128)(2,1)S(1)} %pad_maximum_fusion.9), channel_id=1, source_target_pairs={{0,16},{8,24},{16,0},{24,8},{1,17},{9,25},{17,1},{25,9},{2,18},{10... | collective-permute-start | bytes 1081352 | tf_op jit(solution)/shard_map/ppermute | solution.py:24
  63.8 21.4 %collective-permute-start.42 = (bf16[4,352,128]{2,1,0:T(8,128)(2,1)S(1)}, bf16[4,352,128]{2,1,0:T(8,128)(2,1)S(1)}, u32[]{:S(2)}, u32[]{:S(2)}) collective-permute-start(bf16[4,352,128]{2,1,0:T(8,128)(2,1)S(1)} %pad_maximum_fusion.9), channel_id=1, source_target_pairs={{0,8},{8,16},{16,24},{24,0},{1,9},{9,17},{17,25},{25,1},{2,10},{10... | collective-permute-start | bytes 1081352 | tf_op jit(solution)/shard_map/ppermute | solution.py:24
  77.4 20.8 %collective-permute-start.37 = (bf16[352,512]{1,0:T(8,128)(2,1)S(1)}, bf16[352,512]{1,0:T(8,128)(2,1)S(1)}, u32[]{:S(2)}, u32[]{:S(2)}) collective-permute-start(bf16[352,512]{1,0:T(8,128)(2,1)S(1)} %pad_maximum_fusion.8), channel_id=1, source_target_pairs={{0,96},{32,0},{64,32},{96,64},{1,97},{33,1},{65,33},{97,65},{2,98}... | collective-permute-start | bytes 1081352 | tf_op jit(solution)/shard_map/ppermute | solution.py:24
  85.1 20.3 %collective-permute-start.38 = (bf16[352,512]{1,0:T(8,128)(2,1)S(1)}, bf16[352,512]{1,0:T(8,128)(2,1)S(1)}, u32[]{:S(2)}, u32[]{:S(2)}) collective-permute-start(bf16[352,512]{1,0:T(8,128)(2,1)S(1)} %pad_maximum_fusion.8), channel_id=1, source_target_pairs={{0,64},{32,96},{64,0},{96,32},{1,65},{33,97},{65,1},{97,33},{2,66}... | collective-permute-start | bytes 1081352 | tf_op jit(solution)/shard_map/ppermute | solution.py:24
  85.2 23.7 %collective-permute-start.39 = (bf16[352,512]{1,0:T(8,128)(2,1)S(1)}, bf16[352,512]{1,0:T(8,128)(2,1)S(1)}, u32[]{:S(2)}, u32[]{:S(2)}) collective-permute-start(bf16[352,512]{1,0:T(8,128)(2,1)S(1)} %pad_maximum_fusion.8), channel_id=1, source_target_pairs={{0,32},{32,64},{64,96},{96,0},{1,33},{33,65},{65,97},{97,1},{2,34}... | collective-permute-start | bytes 1081352 | tf_op jit(solution)/shard_map/ppermute | solution.py:24
  98.2 17.5 %collective-permute-start.27 = (bf16[704,512]{1,0:T(8,128)(2,1)S(1)}, bf16[704,512]{1,0:T(8,128)(2,1)S(1)}, u32[]{:S(2)}, u32[]{:S(2)}) collective-permute-start(bf16[704,512]{1,0:T(8,128)(2,1)S(1)} %pad_maximum_fusion.6), channel_id=1, source_target_pairs={{0,32},{32,64},{64,96},{96,0},{1,33},{33,65},{65,97},{97,1},{2,34}... | collective-permute-start | bytes 2162696 | tf_op jit(solution)/shard_map/ppermute | solution.py:24
  105.4 32.6 %collective-permute-start.32 = (bf16[4,704,128]{2,1,0:T(8,128)(2,1)S(1)}, bf16[4,704,128]{2,1,0:T(8,128)(2,1)S(1)}, u32[]{:S(2)}, u32[]{:S(2)}) collective-permute-start(bf16[4,704,128]{2,1,0:T(8,128)(2,1)S(1)} %pad_maximum_fusion.7), channel_id=1, source_target_pairs={{0,24},{8,0},{16,8},{24,16},{1,25},{9,1},{17,9},{25,17},{2,26},{10... | collective-permute-start | bytes 2162696 | tf_op jit(solution)/shard_map/ppermute | solution.py:24
  108.9 29.7 %collective-permute-start.33 = (bf16[4,704,128]{2,1,0:T(8,128)(2,1)S(1)}, bf16[4,704,128]{2,1,0:T(8,128)(2,1)S(1)}, u32[]{:S(2)}, u32[]{:S(2)}) collective-permute-start(bf16[4,704,128]{2,1,0:T(8,128)(2,1)S(1)} %pad_maximum_fusion.7), channel_id=1, source_target_pairs={{0,16},{8,24},{16,0},{24,8},{1,17},{9,25},{17,1},{25,9},{2,18},{10... | collective-permute-start | bytes 2162696 | tf_op jit(solution)/shard_map/ppermute | solution.py:24
  109.5 41.0 %collective-permute-start.16 = (bf16[128,2048]{1,0:T(8,128)(2,1)S(1)}, bf16[128,2048]{1,0:T(8,128)(2,1)S(1)}, u32[]{:S(2)}, u32[]{:S(2)}) collective-permute-start(bf16[128,2048]{1,0:T(8,128)(2,1)S(1)} %get-tuple-element.15.x), channel_id=1, source_target_pairs={{0,6},{2,0},{4,2},{6,4},{1,7},{3,1},{5,3},{7,5},{8,14},{10,8},{12,... | collective-permute-start | bytes 1572872 | tf_op jit(solution)/shard_map/ppermute | solution.py:24
  111.4 30.4 %collective-permute-start.34 = (bf16[4,704,128]{2,1,0:T(8,128)(2,1)S(1)}, bf16[4,704,128]{2,1,0:T(8,128)(2,1)S(1)}, u32[]{:S(2)}, u32[]{:S(2)}) collective-permute-start(bf16[4,704,128]{2,1,0:T(8,128)(2,1)S(1)} %pad_maximum_fusion.7), channel_id=1, source_target_pairs={{0,8},{8,16},{16,24},{24,0},{1,9},{9,17},{17,25},{25,1},{2,10},{10... | collective-permute-start | bytes 2162696 | tf_op jit(solution)/shard_map/ppermute | solution.py:24
  115.7 35.5 %collective-permute-start.12 = (bf16[2048,256]{1,0:T(8,128)(2,1)S(1)}, bf16[2048,256]{1,0:T(8,128)(2,1)S(1)}, u32[]{:S(2)}, u32[]{:S(2)}) collective-permute-start(bf16[2048,256]{1,0:T(8,128)(2,1)S(1)} %pad_maximum_fusion.4.in_own), channel_id=1, source_target_pairs={{0,1},{1,0},{2,3},{3,2},{4,5},{5,4},{6,7},{7,6},{8,9},{9,8},{10,11... | collective-permute-start | bytes 3145736 | tf_op jit(solution)/shard_map/ppermute | solution.py:24
  138.7 71.3 %collective-permute-start.43 = (bf16[704,2048]{1,0:T(8,128)(2,1)S(1)}, bf16[704,2048]{1,0:T(8,128)(2,1)}, u32[]{:S(2)}, u32[]{:S(2)}) collective-permute-start(bf16[704,2048]{1,0:T(8,128)(2,1)S(1)} %pad_maximum_fusion.3), channel_id=1, source_target_pairs={{0,1},{1,0},{2,3},{3,2},{4,5},{5,4},{6,7},{7,6},{8,9},{9,8},{10,11... | collective-permute-start | bytes 8650760 | tf_op jit(solution)/shard_map/ppermute | solution.py:24
  141.8 76.1 %collective-permute-start.28 = (bf16[704,2048]{1,0:T(8,128)(2,1)S(1)}, bf16[704,2048]{1,0:T(8,128)(2,1)}, u32[]{:S(2)}, u32[]{:S(2)}) collective-permute-start(bf16[704,2048]{1,0:T(8,128)(2,1)S(1)} %constant_dynamic-update-slice_fusion.64), channel_id=1, source_target_pairs={{0,1},{1,0},{2,3},{3,2},{4,5},{5,4},{6,7},{7,6},{8,9},{9,8},{10,11... | collective-permute-start | bytes 8650760 | tf_op jit(solution)/shard_map/ppermute | solution.py:24
  150.5 16.3 %collective-permute-start.18 = (bf16[128,2048]{1,0:T(8,128)(2,1)S(1)}, bf16[128,2048]{1,0:T(8,128)(2,1)S(1)}, u32[]{:S(2)}, u32[]{:S(2)}) collective-permute-start(bf16[128,2048]{1,0:T(8,128)(2,1)S(1)} %get-tuple-element.15.x), channel_id=1, source_target_pairs={{0,4},{2,6},{4,0},{6,2},{1,5},{3,7},{5,1},{7,3},{8,12},{10,14},{12... | collective-permute-start | bytes 1572872 | tf_op jit(solution)/shard_map/ppermute | solution.py:24
  151.2 70.3 %collective-permute-start.35 = (bf16[704,2048]{1,0:T(8,128)(2,1)}, bf16[704,2048]{1,0:T(8,128)(2,1)}, u32[]{:S(2)}, u32[]{:S(2)}) collective-permute-start(bf16[704,2048]{1,0:T(8,128)(2,1)} %constant_dynamic-update-slice_fusion.71), channel_id=1, source_target_pairs={{0,1},{1,0},{2,3},{3,2},{4,5},{5,4},{6,7},{7,6},{8,9},{9,8},{10,11... | collective-permute-start | bytes 8650760 | tf_op jit(solution)/shard_map/ppermute | solution.py:24
  151.8 25.7 %collective-permute-start.20 = (bf16[128,2048]{1,0:T(8,128)(2,1)S(1)}, bf16[128,2048]{1,0:T(8,128)(2,1)S(1)}, u32[]{:S(2)}, u32[]{:S(2)}) collective-permute-start(bf16[128,2048]{1,0:T(8,128)(2,1)S(1)} %get-tuple-element.15.x), channel_id=1, source_target_pairs={{0,2},{2,4},{4,6},{6,0},{1,3},{3,5},{5,7},{7,1},{8,10},{10,12},{12... | collective-permute-start | bytes 1572872 | tf_op jit(solution)/shard_map/ppermute | solution.py:24
  166.8 22.4 %collective-permute-start.17 = (bf16[128,2048]{1,0:T(8,128)(2,1)S(1)}, bf16[128,2048]{1,0:T(8,128)(2,1)S(1)}, u32[]{:S(2)}, u32[]{:S(2)}) collective-permute-start(bf16[128,2048]{1,0:T(8,128)(2,1)S(1)} %shard_map.129), channel_id=1, source_target_pairs={{0,2},{2,4},{4,6},{6,0},{1,3},{3,5},{5,7},{7,1},{8,10},{10,12},{12... | collective-permute-start | bytes 1572872 | tf_op jit(solution)/shard_map/ppermute | solution.py:24
  180.5 19.5 %collective-permute-start.19 = (bf16[128,2048]{1,0:T(8,128)(2,1)S(1)}, bf16[128,2048]{1,0:T(8,128)(2,1)S(1)}, u32[]{:S(2)}, u32[]{:S(2)}) collective-permute-start(bf16[128,2048]{1,0:T(8,128)(2,1)S(1)} %shard_map.130), channel_id=1, source_target_pairs={{0,4},{2,6},{4,0},{6,2},{1,5},{3,7},{5,1},{7,3},{8,12},{10,14},{12... | collective-permute-start | bytes 1572872 | tf_op jit(solution)/shard_map/ppermute | solution.py:24
  189.2 16.8 %collective-permute-start.21 = (bf16[128,2048]{1,0:T(8,128)(2,1)S(1)}, bf16[128,2048]{1,0:T(8,128)(2,1)S(1)}, u32[]{:S(2)}, u32[]{:S(2)}) collective-permute-start(bf16[128,2048]{1,0:T(8,128)(2,1)S(1)} %shard_map.131), channel_id=1, source_target_pairs={{0,6},{2,0},{4,2},{6,4},{1,7},{3,1},{5,3},{7,5},{8,14},{10,8},{12,... | collective-permute-start | bytes 1572872 | tf_op jit(solution)/shard_map/ppermute | solution.py:24
  207.3 25.2 %collective-permute-start.44 = (bf16[128,2048]{1,0:T(8,128)(2,1)S(1)}, bf16[128,2048]{1,0:T(8,128)(2,1)}, u32[]{:S(2)}, u32[]{:S(2)}) collective-permute-start(bf16[128,2048]{1,0:T(8,128)(2,1)S(1)} %get-tuple-element.20.x), channel_id=1, source_target_pairs={{0,6},{2,0},{4,2},{6,4},{1,7},{3,1},{5,3},{7,5},{8,14},{10,8},{12,... | collective-permute-start | bytes 1572872 | tf_op jit(solution)/shard_map/ppermute | solution.py:24
  210.0 33.6 %collective-permute-start.46 = (bf16[128,2048]{1,0:T(8,128)(2,1)S(1)}, bf16[128,2048]{1,0:T(8,128)(2,1)}, u32[]{:S(2)}, u32[]{:S(2)}) collective-permute-start(bf16[128,2048]{1,0:T(8,128)(2,1)S(1)} %get-tuple-element.20.x), channel_id=1, source_target_pairs={{0,4},{2,6},{4,0},{6,2},{1,5},{3,7},{5,1},{7,3},{8,12},{10,14},{12... | collective-permute-start | bytes 1572872 | tf_op jit(solution)/shard_map/ppermute | solution.py:24
  210.0 47.3 %collective-permute-start.48 = (bf16[128,2048]{1,0:T(8,128)(2,1)S(1)}, bf16[128,2048]{1,0:T(8,128)(2,1)S(1)}, u32[]{:S(2)}, u32[]{:S(2)}) collective-permute-start(bf16[128,2048]{1,0:T(8,128)(2,1)S(1)} %get-tuple-element.20.x), channel_id=1, source_target_pairs={{0,2},{2,4},{4,6},{6,0},{1,3},{3,5},{5,7},{7,1},{8,10},{10,12},{12... | collective-permute-start | bytes 1572872 | tf_op jit(solution)/shard_map/ppermute | solution.py:24
  243.5 28.3 %collective-permute-start.45 = (bf16[128,2048]{1,0:T(8,128)(2,1)S(1)}, bf16[128,2048]{1,0:T(8,128)(2,1)S(1)}, u32[]{:S(2)}, u32[]{:S(2)}) collective-permute-start(bf16[128,2048]{1,0:T(8,128)(2,1)S(1)} %shard_map.137), channel_id=1, source_target_pairs={{0,2},{2,4},{4,6},{6,0},{1,3},{3,5},{5,7},{7,1},{8,10},{10,12},{12... | collective-permute-start | bytes 1572872 | tf_op jit(solution)/shard_map/ppermute | solution.py:24
  251.9 19.9 %collective-permute-start.47 = (bf16[128,2048]{1,0:T(8,128)(2,1)S(1)}, bf16[128,2048]{1,0:T(8,128)(2,1)S(1)}, u32[]{:S(2)}, u32[]{:S(2)}) collective-permute-start(bf16[128,2048]{1,0:T(8,128)(2,1)S(1)} %shard_map.139), channel_id=1, source_target_pairs={{0,4},{2,6},{4,0},{6,2},{1,5},{3,7},{5,1},{7,3},{8,12},{10,14},{12... | collective-permute-start | bytes 1572872 | tf_op jit(solution)/shard_map/ppermute | solution.py:24
  (37 other events, 367.4 us)
where the time goes:
time: 281 us
  waiting for transfers between devices  119 us (42%)
  starting transfers between devices  72.6 us (26%)
  Pallas kernels  45.7 us (16%)
  local copies, waits for them, and re-layouts  23.6 us (8%)
  other arithmetic  18.8 us (7%)
    ppermute x50, waiting for transfers between devices, fetch(): return lax.ppermute(a, axis, [(i, (i - ahead) % size) for i in range(size)])  119 us
    ppermute x50, starting transfers between devices, fetch(): return lax.ppermute(a, axis, [(i, (i - ahead) % size) for i in range(size)])  72.6 us
    pallas_call x16, Pallas kernels, call(): pl.pallas_call(body, in_specs=[SM] * scalars + [VM] * (len(args) - scalar...  45.7 us
    unnamed x99, local copies, waits for them, and re-layouts  21.5 us
    concatenate x1, other arithmetic, layer(): down = jnp.concatenate([down, partner(down)], axis=0)  7 us
    concatenate x1, other arithmetic, layer(): val = jnp.concatenate([val, partner(val)], axis=0)  6.16 us
  transfers between devices with their start and end apart: 50, of which 18 were waited for; matrix products, arithmetic and copies ran while one was open for 11% of the time, Pallas kernels for 15%

commit v1 on v0

--- a/solution.py
+++ b/solution.py
@@ -34,18 +34,18 @@
 
 VM = pl.BlockSpec(memory_space=pltpu.VMEM)
 SM = pl.BlockSpec(memory_space=pltpu.SMEM)
-
-
-def call(body, out, *args, vmem=4, scalars=0, flops=0, scratch=()):
+ANY = pl.BlockSpec(memory_space=pl.ANY)
+
+
+def call(body, out, *args, vmem=4, scalars=0, flops=0, scratch=(), where=VM):
     return pl.pallas_call(
         body,
-        in_specs=[SM] * scalars + [VM] * (len(args) - scalars),
+        in_specs=[SM] * scalars + [where] * (len(args) - scalars),
+        out_specs=jax.tree.map(lambda _: VM, out),
         out_shape=out,
-        scratch_shapes=[pltpu.VMEM(*v) for v in scratch],
+        scratch_shapes=scratch,
         compiler_params=pltpu.CompilerParams(vmem_limit_bytes=vmem * MIB),
-        cost_estimate=pl.CostEstimate(
-            flops=flops, transcendentals=0, bytes_accessed=0
-        ),
+        cost_estimate=pl.CostEstimate(flops=flops, transcendentals=0, bytes_accessed=0),
     )(*args)
 
 
@@ -53,7 +53,32 @@
     return jax.ShapeDtypeStruct(shape, dtype)
 
 
-def first_body(order, resid, gain, gain2, in_w, out_w, resid_rel, normed_rel, gain2_rel, a, b):
+def first_body(
+    order, resid_h, gain_h, gain2_h, in_h, out_h, gate_h, val_h, down_h,
+    resid_rel, normed_rel, gain2_rel, a, b, resid, gain, gain2, sems,
+):
+    copies = [
+        pltpu.make_async_copy(src, dst, sems.at[i])
+        for i, (src, dst) in enumerate(
+            [
+                (resid_h, resid),
+                (gain_h, gain),
+                (gain2_h, gain2),
+                (in_h.at[:, :BLK], a.at[:BLK]),
+                (in_h.at[:, BLK:], b.at[:BLK]),
+                (out_h.at[:BLK], a.at[BLK : 2 * BLK]),
+                (out_h.at[BLK:], b.at[BLK : 2 * BLK]),
+                (gate_h, a.at[256 : 256 + HID]),
+                (val_h, b.at[256 : 256 + HID]),
+                (down_h.at[: HID // 2], a.at[256 + HID :]),
+                (down_h.at[HID // 2 :], b.at[256 + HID :]),
+            ]
+        )
+    ]
+    for c in copies:
+        c.start()
+    for c in copies[:3]:
+        c.wait()
     wide = resid[...].astype(F32)
     scale = lax.rsqrt(jnp.mean(wide * wide, axis=-1, keepdims=True) + 1e-06)
     for j in range(D // BLK):
@@ -63,16 +88,8 @@
         resid_rel[:, put] = block
         normed_rel[:, put] = (block.astype(F32) * scale * gain[:, pl.ds(at, BLK)]).astype(BF16)
         gain2_rel[:, put] = gain2[:, pl.ds(at, BLK)]
-    for half, dst in enumerate((a, b)):
-        dst[:BLK] = in_w[:, half * BLK : (half + 1) * BLK]
-        dst[BLK:] = out_w[half * BLK : (half + 1) * BLK]
-
-
-def halves_body(gate, val, down, a, b):
-    a[:HID] = gate[...]
-    a[HID:] = down[: HID // 2]
-    b[:HID] = val[...]
-    b[HID:] = down[HID // 2 :]
+    for c in copies[3:]:
+        c.wait()
 
 
 def second_norm_body(resid, p0, p1, p2, p3, gain, middle, normed):
@@ -154,21 +171,40 @@
     return lax.dot_general(a, b, (((1,), (1,)), ((), ())), preferred_element_type=F32)
 
 
-def up_body(x, gate, val, taps, out):
+def tick_body(taps, out):
+    out[...] = taps[...]
+
+
+def up_body(x, gate, val, taps, out, buf):
     rows = lax.broadcasted_iota(jnp.int32, (SEQ, BLK), 0)
-
-    def tile(t, carry):
+    last = 2 * HID // BLK - 1
+
+    def product(t):
         cols = pl.ds(pl.multiple_of(t * BLK, BLK), BLK)
-        both = nt_dot(x[...], jnp.concatenate([gate[cols], val[cols]], axis=0))
+        return nt_dot(x[...], jnp.concatenate([gate[cols], val[cols]], axis=0))
+
+    def finish(t, both):
+        cols = pl.ds(pl.multiple_of(t * BLK, BLK), BLK)
         both = both.astype(BF16).astype(F32)
         g, v = both[:, :BLK], both[:, BLK:]
         conv = g * taps[2:3, cols]
         for k in range(2):
             conv = conv + delayed(g, 2 - k, rows, 0.0) * taps[k : k + 1, cols]
         out[:, cols] = (conv * sigmoid(conv) * v).astype(BF16)
+
+    buf[0] = product(0)
+
+    def tile(i, carry):
+        t = 2 * i
+        one = product(t + 1)
+        finish(t, buf[0])
+        two = product(t + 2)
+        finish(t + 1, one)
+        buf[0] = two
         return carry
 
-    lax.fori_loop(0, 2 * HID // BLK, tile, 0)
+    lax.fori_loop(0, last // 2, tile, 0)
+    finish(last, buf[0])
 
 
 def down_body(h, down, out):
@@ -184,8 +220,11 @@
     return fetch(part, "y", (-ahead) % 4)
 
 
-def in_lanes(pieces):
-    return jnp.concatenate(pieces, axis=1)
+def placed(shape, blocks):
+    out = jnp.zeros(shape, BF16)
+    for piece, r, c in blocks:
+        out = lax.dynamic_update_slice(out, piece, (r, c))
+    return out
 
 
 def layer(
@@ -207,33 +246,60 @@
     steps = jnp.arange(16, dtype=jnp.int32)
     order = ((steps // 4 + z) % 4) * 4 + (steps % 4 + x) % 4
 
+    half = sds((256 + HID + HID // 2, BLK))
     resid_rel, normed, gain2, a, b = call(
         first_body,
-        [sds((SEQ, D)), sds((SEQ, D)), sds((1, D), F32), sds((256, BLK)), sds((256, BLK))],
+        [sds((SEQ, D)), sds((SEQ, D)), sds((1, D), F32), half, half],
         order,
         resid,
         mix_gain.reshape(1, D),
         mlp_gain.reshape(1, D),
         in_weight,
         out_weight,
+        up_gate_w.T,
+        up_val_w.T,
+        down_weight,
         scalars=1,
+        where=ANY,
+        scratch=[
+            pltpu.VMEM((SEQ, D), BF16),
+            pltpu.VMEM((1, D), F32),
+            pltpu.VMEM((1, D), F32),
+            pltpu.SemaphoreType.DMA((11,)),
+        ],
     )
     rows1 = fetch_all(normed, "y")
 
-    a = jnp.stack(fetch_all(a, "x"))
-    b = jnp.stack(fetch_all(b, "z"))
-    a = fetch_all(a, "z")
-    b = fetch_all(b, "x")
-    a = [a[i][j] for i in range(4) for j in range(4)]
-    b = [b[j][i] for i in range(4) for j in range(4)]
-    in_own = jnp.concatenate(
-        [jnp.concatenate([v[:BLK] for v in h], axis=0) for h in (a, b)], axis=1
-    )
-    out_own = jnp.concatenate([in_lanes([v[BLK:] for v in h]) for h in (a, b)], axis=0)
+    a = fetch_all(a, "x")
+    b = fetch_all(b, "z")
+    pa = fetch_all(jnp.stack([v[:256] for v in a]), "z")
+    pb = fetch_all(jnp.stack([v[:256] for v in b]), "x")
+    ua = jnp.concatenate([v[256:] for v in a], axis=1)
+    ub = jnp.stack([v[256:] for v in b])
+    ua = fetch_all(ua, "z")
+    ub = fetch_all(ub, "x")
+    near = [(i, j, (4 * i + j) * BLK) for i in range(4) for j in range(4)]
+    in_own = placed(
+        (D, 256),
+        [(pa[i][j, :BLK], at, 0) for i, j, at in near]
+        + [(pb[j][i, :BLK], at, BLK) for i, j, at in near],
+    )
+    out_own = placed(
+        (256, D),
+        [(pa[i][j, BLK:], 0, at) for i, j, at in near]
+        + [(pb[j][i, BLK:], BLK, at) for i, j, at in near],
+    )
     in_par, out_par = partner(in_own), partner(out_own)
 
-    gates = jnp.stack([recur_gate_w, input_gate_w])
-    gates = jnp.concatenate([gates, partner(gates)], axis=1).reshape(2, 4, 2, 64, 64)
+    (rgw, igw, small, rate, ftaps_own), _ = lax.optimization_barrier(
+        ((recur_gate_w, input_gate_w, conv_taps, decay_rate[None], ffn_taps), a[1])
+    )
+    gates = jnp.stack(
+        [
+            jnp.concatenate([rgw, partner(rgw)], axis=0),
+            jnp.concatenate([igw, partner(igw)], axis=0),
+        ]
+    ).reshape(2, 4, 2, 64, 64)
     zero = jnp.zeros_like(gates[:, :, 0])
     gates = jnp.concatenate(
         [
@@ -243,26 +309,26 @@
         axis=2,
     )
     gates = jnp.concatenate([gates[0], gates[1]], axis=2)
-    small = jnp.concatenate([conv_taps, decay_rate[None]], axis=0)
-    small = jnp.concatenate([small, partner(small)], axis=1)
-    taps, rate = small[:4], small[4:]
-    ftaps = jnp.concatenate([ffn_taps, partner(ffn_taps)], axis=1)
-
-    a, b = call(
-        halves_body, [sds((1056, BLK)), sds((1056, BLK))], up_gate_w.T, up_val_w.T, down_weight
-    )
-    a = fetch_all(a, "x")
-    b = fetch_all(b, "z")
-    gate = in_lanes(fetch_all(in_lanes([v[:HID] for v in a]), "z"))
-    val = fetch_all(jnp.stack([v[:HID] for v in b]), "x")
-    val = in_lanes([val[j][i] for i in range(4) for j in range(4)])
-    down_a = in_lanes(fetch_all(in_lanes([v[HID:] for v in a]), "z"))
-    down_b = fetch_all(jnp.stack([v[HID:] for v in b]), "x")
-    down_b = in_lanes([down_b[j][i] for i in range(4) for j in range(4)])
-    down = jnp.concatenate([down_a, down_b], axis=0)
-    gate = jnp.concatenate([gate, partner(gate)], axis=0)
-    val = jnp.concatenate([val, partner(val)], axis=0)
-    down = jnp.concatenate([down, partner(down)], axis=0)
+    taps = jnp.concatenate([small, partner(small)], axis=1)
+    rate = jnp.concatenate([rate, partner(rate)], axis=1)
+    ftaps_par = partner(ftaps_own)
+    ftaps = jnp.concatenate([ftaps_own, ftaps_par], axis=1)
+
+    ua_par = [partner(v) for v in ua]
+    ub_par = [partner(v) for v in ub]
+    gate, val, down = [], [], []
+    for c, (wa, wb) in enumerate(((ua, ub), (ua_par, ub_par))):
+        top = c * HID
+        for k in (0, 1, 3, 2):
+            gate.append((wa[k][:HID], top, k * 512))
+            down.append((wa[k][HID:], top, k * 512))
+            for i in range(4):
+                at = (4 * i + k) * BLK
+                val.append((wb[k][i, :HID], top, at))
+                down.append((wb[k][i, HID:], top + HID // 2, at))
+    gate = placed((2 * HID, D), gate)
+    val = placed((2 * HID, D), val)
+    down = placed((2 * HID, D), down)
 
     parts = [None] * 4
     for j in (1, 3, 2, 0):
@@ -278,16 +344,24 @@
             out_own,
             out_par,
             flops=2 * SEQ * D * 512 * 2,
-            scratch=[((SEQ, 512), BF16), ((SEQ, 512), BF16)],
+            scratch=[pltpu.VMEM((SEQ, 512), BF16)] * 2,
         )
         parts[j] = sums_sent(part, j) if j else part
     middle, normed_two = call(
         second_norm_body, [sds((SEQ, D)), sds((SEQ, D))], resid_rel, *parts, gain2
     )
     rows2 = fetch_all(normed_two, "y")
+    ftaps = call(tick_body, sds((3, 2 * HID), F32), ftaps)
     for j in (0, 1, 3, 2):
         hidden = call(
-            up_body, sds((SEQ, 2 * HID)), rows2[j], gate, val, ftaps, flops=2 * SEQ * D * 1408 * 2
+            up_body,
+            sds((SEQ, 2 * HID)),
+            rows2[j],
+            gate,
+            val,
+            ftaps,
+            flops=2 * SEQ * D * 1408 * 2,
+            scratch=[pltpu.VMEM((1, SEQ, 256), F32)],
         )
         part = call(down_body, sds((SEQ, D)), hidden, down, flops=2 * SEQ * D * 1408)
         parts[j] = sums_sent(part, j) if j else part

time: 281 us -> 281 us (level)
  the two profiles are of different devices: /device:TPU:32 before, /device:TPU:1 now
where the time goes in v1:
time: 281 us
  waiting for transfers between devices  154 us (55%)
  starting transfers between devices  69.6 us (25%)
  Pallas kernels  41.2 us (15%)
  local copies, waits for them, and re-layouts  13.7 us (5%)
    ppermute x45, waiting for transfers between devices, fetch(): return lax.ppermute(a, axis, [(i, (i - ahead) % size) for i in range(size)])  154 us
    ppermute x45, starting transfers between devices, fetch(): return lax.ppermute(a, axis, [(i, (i - ahead) % size) for i in range(size)])  69.6 us
    pallas_call x16, Pallas kernels, call(): pl.pallas_call(body, in_specs=[SM] * scalars + [where] * (len(args) - sca...  41.2 us
    unnamed x28, local copies, waits for them, and re-layouts  6.91 us
    dynamic_update_slice x113, local copies, waits for them, and re-layouts, placed(): out = lax.dynamic_update_slice(out, piece, (r, c))  6.45 us
  transfers between devices with their start and end apart: 45, of which 25 were waited for; matrix products, arithmetic and copies ran while one was open for 3% of the time, Pallas kernels for 11%

profile of v1, /device:TPU:1, one launch (start us, length us, event | category | flops | bytes accessed | tf_op | source)
XLA Modules:
  0.0 280.6 jit_solution(3031275801558040033)
XLA Ops:
  16.1 3.3 %collective-permute-start.7 = (bf16[1312,128]{1,0:T(8,128)(2,1)S(1)}, bf16[1312,128]{1,0:T(8,128)(2,1)S(1)}, u32[]{:S(2)}, u32[]{:S(2)}) collective-permute-start(bf16[1312,128]{1,0:T(8,128)(2,1)S(1)} %get-tuple-element.20), channel_id=1, source_target_pairs={{0,64},{32,96},{64,0},{96,32},{1,65},{33,97},{65,1},{97,33},{2,66}... | collective-permute-start | bytes 1007624 | tf_op jit(solution)/shard_map/ppermute | solution.py:24
  20.5 6.9 %collective-permute-done = bf16[1312,128]{1,0:T(8,128)(2,1)S(1)} collective-permute-done((bf16[1312,128]{1,0:T(8,128)(2,1)S(1)}, bf16[1312,128]{1,0:T(8,128)(2,1)S(1)}, u32[]{:S(2)}, u32[]{:S(2)}) %collective-permute-start) | collective-permute-done | bytes 335904 | tf_op jit(solution)/shard_map/ppermute | solution.py:24
  27.4 3.9 %collective-permute-start.6 = (bf16[1312,128]{1,0:T(8,128)(2,1)S(1)}, bf16[1312,128]{1,0:T(8,128)(2,1)S(1)}, u32[]{:S(2)}, u32[]{:S(2)}) collective-permute-start(bf16[1312,128]{1,0:T(8,128)(2,1)S(1)} %get-tuple-element.20), channel_id=1, source_target_pairs={{0,96},{32,0},{64,32},{96,64},{1,97},{33,1},{65,33},{97,65},{2,98}... | collective-permute-start | bytes 1007624 | tf_op jit(solution)/shard_map/ppermute | solution.py:24
  32.7 2.7 collective-permute-start.20
  37.5 2.8 collective-permute-start.16
  47.4 5.0 %collective-permute-done.3 = bf16[4,256,128]{2,1,0:T(8,128)(2,1)S(1)} collective-permute-done((bf16[4,256,128]{2,1,0:T(8,128)(2,1)S(1)}, bf16[4,256,128]{2,1,0:T(8,128)(2,1)S(1)}, u32[]{:S(2)}, u32[]{:S(2)}) %collective-permute-start.3) | collective-permute-done | bytes 262176 | tf_op jit(solution)/shard_map/ppermute | solution.py:24
  55.2 5.4 %collective-permute-done.4 = bf16[4,256,128]{2,1,0:T(8,128)(2,1)S(1)} collective-permute-done((bf16[4,256,128]{2,1,0:T(8,128)(2,1)S(1)}, bf16[4,256,128]{2,1,0:T(8,128)(2,1)S(1)}, u32[]{:S(2)}, u32[]{:S(2)}) %collective-permute-start.4) | collective-permute-done | bytes 262176 | tf_op jit(solution)/shard_map/ppermute | solution.py:24
  65.1 10.7 %collective-permute-done.9 = bf16[4,256,128]{2,1,0:T(8,128)(2,1)S(1)} collective-permute-done((bf16[4,256,128]{2,1,0:T(8,128)(2,1)S(1)}, bf16[4,256,128]{2,1,0:T(8,128)(2,1)S(1)}, u32[]{:S(2)}, u32[]{:S(2)}) %collective-permute-start.9) | collective-permute-done | bytes 262176 | tf_op jit(solution)/shard_map/ppermute | solution.py:24
  77.6 3.5 %collective-permute-start.24 = (bf16[1056,512]{1,0:T(8,128)(2,1)S(1)}, bf16[1056,512]{1,0:T(8,128)(2,1)S(1)}, u32[]{:S(2)}, u32[]{:S(2)}) collective-permute-start(bf16[1056,512]{1,0:T(8,128)(2,1)S(1)} %pad_maximum_fusion), channel_id=1, source_target_pairs={{0,96},{32,0},{64,32},{96,64},{1,97},{33,1},{65,33},{97,65},{2,98}... | collective-permute-start | bytes 3244040 | tf_op jit(solution)/shard_map/ppermute | solution.py:24
  81.1 3.6 %collective-permute-done.11 = bf16[4,256,128]{2,1,0:T(8,128)(2,1)S(1)} collective-permute-done((bf16[4,256,128]{2,1,0:T(8,128)(2,1)S(1)}, bf16[4,256,128]{2,1,0:T(8,128)(2,1)S(1)}, u32[]{:S(2)}, u32[]{:S(2)}) %collective-permute-start.11) | collective-permute-done | bytes 262176 | tf_op jit(solution)/shard_map/ppermute | solution.py:24
  86.9 16.5 %collective-permute-done.24 = bf16[1056,512]{1,0:T(8,128)(2,1)S(1)} collective-permute-done((bf16[1056,512]{1,0:T(8,128)(2,1)S(1)}, bf16[1056,512]{1,0:T(8,128)(2,1)S(1)}, u32[]{:S(2)}, u32[]{:S(2)}) %collective-permute-start.24) | collective-permute-done | bytes 1081376 | tf_op jit(solution)/shard_map/ppermute | solution.py:24
  103.9 4.5 %collective-permute-done.31 = bf16[4,1056,128]{2,1,0:T(8,128)(2,1)S(1)} collective-permute-done((bf16[4,1056,128]{2,1,0:T(8,128)(2,1)S(1)}, bf16[4,1056,128]{2,1,0:T(8,128)(2,1)S(1)}, u32[]{:S(2)}, u32[]{:S(2)}) %collective-permute-start.31) | collective-permute-done | bytes 1081376 | tf_op jit(solution)/shard_map/ppermute | solution.py:24
  108.8 20.4 %collective-permute-done.25 = bf16[1056,512]{1,0:T(8,128)(2,1)S(1)} collective-permute-done((bf16[1056,512]{1,0:T(8,128)(2,1)S(1)}, bf16[1056,512]{1,0:T(8,128)(2,1)S(1)}, u32[]{:S(2)}, u32[]{:S(2)}) %collective-permute-start.25) | collective-permute-done | bytes 1081376 | tf_op jit(solution)/shard_map/ppermute | solution.py:24
  129.5 4.1 %collective-permute-done.32 = bf16[4,1056,128]{2,1,0:T(8,128)(2,1)S(1)} collective-permute-done((bf16[4,1056,128]{2,1,0:T(8,128)(2,1)S(1)}, bf16[4,1056,128]{2,1,0:T(8,128)(2,1)S(1)}, u32[]{:S(2)}, u32[]{:S(2)}) %collective-permute-start.32) | collective-permute-done | bytes 1081376 | tf_op jit(solution)/shard_map/ppermute | solution.py:24
  134.0 19.8 %collective-permute-done.26 = bf16[1056,512]{1,0:T(8,128)(2,1)S(1)} collective-permute-done((bf16[1056,512]{1,0:T(8,128)(2,1)S(1)}, bf16[1056,512]{1,0:T(8,128)(2,1)S(1)}, u32[]{:S(2)}, u32[]{:S(2)}) %collective-permute-start.26) | collective-permute-done | bytes 1081376 | tf_op jit(solution)/shard_map/ppermute | solution.py:24
  153.8 3.2 %collective-permute-start.34 = (bf16[4,1056,128]{2,1,0:T(8,128)(2,1)S(1)}, bf16[4,1056,128]{2,1,0:T(8,128)(2,1)S(1)}, u32[]{:S(2)}, u32[]{:S(2)}) collective-permute-start(bf16[4,1056,128]{2,1,0:T(8,128)(2,1)S(1)} %pad_maximum_fusion.1), channel_id=1, source_target_pairs={{0,1},{1,0},{2,3},{3,2},{4,5},{5,4},{6,7},{7,6},{8,9},{9,8},{10,11... | collective-permute-start | bytes 3244040 | tf_op jit(solution)/shard_map/ppermute | solution.py:24
  157.7 3.7 %collective-permute-start.27 = (bf16[1056,512]{1,0:T(8,128)(2,1)S(1)}, bf16[1056,512]{1,0:T(8,128)(2,1)S(1)}, u32[]{:S(2)}, u32[]{:S(2)}) collective-permute-start(bf16[1056,512]{1,0:T(8,128)(2,1)S(1)} %pad_maximum_fusion), channel_id=1, source_target_pairs={{0,1},{1,0},{2,3},{3,2},{4,5},{5,4},{6,7},{7,6},{8,9},{9,8},{10,11... | collective-permute-start | bytes 3244040 | tf_op jit(solution)/shard_map/ppermute | solution.py:24
  166.7 2.8 %shard_map.129 = bf16[128,2048]{1,0:T(8,128)(2,1)S(1)} custom-call(bf16[128,2048]{1,0:T(8,128)(2,1)S(1)} %collective-permute-done.18.x, bf16[2048,256]{1,0:T(8,128)(2,1)S(1)} %get-tuple-element.30.in_own, bf16[2048,256]{1,0:T(8,128)(2,1)S(1)} %collective-permute-done.12.in_par, f32[4,512]{1,0:T(4,128)S(1)} %constant_dynamic-update-slice_fusion.taps, ...), custom_call_target="tpu_custom_call" | custom-call | flops 536870912 | tf_op jit(solution)/shard_map/pallas_call | solution.py:41
  171.0 2.9 %shard_map.130 = bf16[128,2048]{1,0:T(8,128)(2,1)S(1)} custom-call(bf16[128,2048]{1,0:T(8,128)(2,1)S(1)} %collective-permute-done.20.x, bf16[2048,256]{1,0:T(8,128)(2,1)S(1)} %get-tuple-element.30.in_own, bf16[2048,256]{1,0:T(8,128)(2,1)S(1)} %collective-permute-done.12.in_par, f32[4,512]{1,0:T(4,128)S(1)} %constant_dynamic-update-slice_fusion.taps, ...), custom_call_target="tpu_custom_call" | custom-call | flops 536870912 | tf_op jit(solution)/shard_map/pallas_call | solution.py:41
  173.8 2.7 collective-permute-start.21
  176.5 2.8 %shard_map.131 = bf16[128,2048]{1,0:T(8,128)(2,1)S(1)} custom-call(bf16[128,2048]{1,0:T(8,128)(2,1)S(1)} %collective-permute-done.22.x, bf16[2048,256]{1,0:T(8,128)(2,1)S(1)} %get-tuple-element.30.in_own, bf16[2048,256]{1,0:T(8,128)(2,1)S(1)} %collective-permute-done.12.in_par, f32[4,512]{1,0:T(4,128)S(1)} %constant_dynamic-update-slice_fusion.taps, ...), custom_call_target="tpu_custom_call" | custom-call | flops 536870912 | tf_op jit(solution)/shard_map/pallas_call | solution.py:41
  180.7 2.9 %shard_map.128.p0 = bf16[128,2048]{1,0:T(8,128)(2,1)S(1)} custom-call(bf16[128,2048]{1,0:T(8,128)(2,1)S(1)} %get-tuple-element.18.x, bf16[2048,256]{1,0:T(8,128)(2,1)S(1)} %get-tuple-element.30.in_own, bf16[2048,256]{1,0:T(8,128)(2,1)S(1)} %collective-permute-done.12.in_par, f32[4,512]{1,0:T(4,128)S(1)} %constant_dynamic-update-slice_fusion.taps, ...), custom_call_target="tpu_custom_call" | custom-call | flops 536870912 | tf_op jit(solution)/shard_map/pallas_call | solution.py:41
  185.3 11.2 %collective-permute-done.21.p2 = bf16[128,2048]{1,0:T(8,128)(2,1)S(1)} collective-permute-done((bf16[128,2048]{1,0:T(8,128)(2,1)S(1)}, bf16[128,2048]{1,0:T(8,128)(2,1)S(1)}, u32[]{:S(2)}, u32[]{:S(2)}) %collective-permute-start.21) | collective-permute-done | bytes 524320 | tf_op jit(solution)/shard_map/ppermute | solution.py:24
  204.0 2.8 %collective-permute-start.41 = (bf16[128,2048]{1,0:T(8,128)(2,1)S(1)}, bf16[128,2048]{1,0:T(8,128)(2,1)S(1)}, u32[]{:S(2)}, u32[]{:S(2)}) collective-permute-start(bf16[128,2048]{1,0:T(8,128)(2,1)S(1)} %get-tuple-element.27.x), channel_id=1, source_target_pairs={{0,4},{2,6},{4,0},{6,2},{1,5},{3,7},{5,1},{7,3},{8,12},{10,14},{12... | collective-permute-start | bytes 1572872 | tf_op jit(solution)/shard_map/ppermute | solution.py:24
  210.3 19.5 %collective-permute-done.39.x = bf16[128,2048]{1,0:T(8,128)(2,1)S(1)} collective-permute-done((bf16[128,2048]{1,0:T(8,128)(2,1)S(1)}, bf16[128,2048]{1,0:T(8,128)(2,1)S(1)}, u32[]{:S(2)}, u32[]{:S(2)}) %collective-permute-start.39) | collective-permute-done | bytes 524320 | tf_op jit(solution)/shard_map/ppermute | solution.py:24
  229.8 4.8 %shard_map.136.h = bf16[128,1408]{1,0:T(8,128)(2,1)S(1)} custom-call(bf16[128,2048]{1,0:T(8,128)(2,1)S(1)} %collective-permute-done.39.x, bf16[1408,2048]{1,0:T(8,128)(2,1)S(1)} %slice_dynamic-update-slice_fusion.gate, bf16[1408,2048]{1,0:T(8,128)(2,1)S(1)} %fusion.3.val, f32[3,1408]{1,0:T(4,128)S(1)} %shard_map.133.taps), custom_call_target="tpu_custom_call" | custom-call | flops 1476395008 | tf_op jit(solution)/shard_map/pallas_call | solution.py:41
  236.2 4.8 %shard_map.138.h = bf16[128,1408]{1,0:T(8,128)(2,1)S(1)} custom-call(bf16[128,2048]{1,0:T(8,128)(2,1)S(1)} %collective-permute-done.41.x, bf16[1408,2048]{1,0:T(8,128)(2,1)S(1)} %slice_dynamic-update-slice_fusion.gate, bf16[1408,2048]{1,0:T(8,128)(2,1)S(1)} %fusion.3.val, f32[3,1408]{1,0:T(4,128)S(1)} %shard_map.133.taps), custom_call_target="tpu_custom_call" | custom-call | flops 1476395008 | tf_op jit(solution)/shard_map/pallas_call | solution.py:41
  242.7 4.8 %shard_map.140.h = bf16[128,1408]{1,0:T(8,128)(2,1)S(1)} custom-call(bf16[128,2048]{1,0:T(8,128)(2,1)S(1)} %collective-permute-done.43.x, bf16[1408,2048]{1,0:T(8,128)(2,1)S(1)} %slice_dynamic-update-slice_fusion.gate, bf16[1408,2048]{1,0:T(8,128)(2,1)S(1)} %fusion.3.val, f32[3,1408]{1,0:T(4,128)S(1)} %shard_map.133.taps), custom_call_target="tpu_custom_call" | custom-call | flops 1476395008 | tf_op jit(solution)/shard_map/pallas_call | solution.py:41
  249.0 3.2 %collective-permute-start.44 = (bf16[128,2048]{1,0:T(8,128)(2,1)S(1)}, bf16[128,2048]{1,0:T(8,128)(2,1)S(1)}, u32[]{:S(2)}, u32[]{:S(2)}) collective-permute-start(bf16[128,2048]{1,0:T(8,128)(2,1)S(1)} %shard_map.141), channel_id=1, source_target_pairs={{0,6},{2,0},{4,2},{6,4},{1,7},{3,1},{5,3},{7,5},{8,14},{10,8},{12,... | collective-permute-start | bytes 1572872 | tf_op jit(solution)/shard_map/ppermute | solution.py:24
  253.0 4.8 %shard_map.134.h = bf16[128,1408]{1,0:T(8,128)(2,1)S(1)} custom-call(bf16[128,2048]{1,0:T(8,128)(2,1)S(1)} %get-tuple-element.27.x, bf16[1408,2048]{1,0:T(8,128)(2,1)S(1)} %slice_dynamic-update-slice_fusion.gate, bf16[1408,2048]{1,0:T(8,128)(2,1)S(1)} %fusion.3.val, f32[3,1408]{1,0:T(4,128)S(1)} %shard_map.133.taps), custom_call_target="tpu_custom_call" | custom-call | flops 1476395008 | tf_op jit(solution)/shard_map/pallas_call | solution.py:41
  259.4 4.5 %collective-permute-done.44.p3 = bf16[128,2048]{1,0:T(8,128)(2,1)S(1)} collective-permute-done((bf16[128,2048]{1,0:T(8,128)(2,1)S(1)}, bf16[128,2048]{1,0:T(8,128)(2,1)S(1)}, u32[]{:S(2)}, u32[]{:S(2)}) %collective-permute-start.44) | collective-permute-done | bytes 524320 | tf_op jit(solution)/shard_map/ppermute | solution.py:24
  266.5 12.3 %collective-permute-done.40.p1 = bf16[128,2048]{1,0:T(8,128)(2,1)S(1)} collective-permute-done((bf16[128,2048]{1,0:T(8,128)(2,1)S(1)}, bf16[128,2048]{1,0:T(8,128)(2,1)S(1)}, u32[]{:S(2)}, u32[]{:S(2)}) %collective-permute-start.40) | collective-permute-done | bytes 524320 | tf_op jit(solution)/shard_map/ppermute | solution.py:24
  (249 shorter events, 72.2 us)
Async XLA Ops:
  8.8 22.5 %collective-permute-start.2 = (bf16[1312,128]{1,0:T(8,128)(2,1)S(1)}, bf16[1312,128]{1,0:T(8,128)(2,1)S(1)}, u32[]{:S(2)}, u32[]{:S(2)}) collective-permute-start(bf16[1312,128]{1,0:T(8,128)(2,1)S(1)} %get-tuple-element.19), channel_id=1, source_target_pairs={{0,8},{8,16},{16,24},{24,0},{1,9},{9,17},{17,25},{25,1},{2,10},{10... | collective-permute-start | bytes 1007624 | tf_op jit(solution)/shard_map/ppermute | solution.py:24
  10.9 21.8 %collective-permute-start.1 = (bf16[1312,128]{1,0:T(8,128)(2,1)S(1)}, bf16[1312,128]{1,0:T(8,128)(2,1)S(1)}, u32[]{:S(2)}, u32[]{:S(2)}) collective-permute-start(bf16[1312,128]{1,0:T(8,128)(2,1)S(1)} %get-tuple-element.19), channel_id=1, source_target_pairs={{0,16},{8,24},{16,0},{24,8},{1,17},{9,25},{17,1},{25,9},{2,18},{10... | collective-permute-start | bytes 1007624 | tf_op jit(solution)/shard_map/ppermute | solution.py:24
  13.3 14.0 %collective-permute-start = (bf16[1312,128]{1,0:T(8,128)(2,1)S(1)}, bf16[1312,128]{1,0:T(8,128)(2,1)S(1)}, u32[]{:S(2)}, u32[]{:S(2)}) collective-permute-start(bf16[1312,128]{1,0:T(8,128)(2,1)S(1)} %get-tuple-element.19), channel_id=1, source_target_pairs={{0,24},{8,0},{16,8},{24,16},{1,25},{9,1},{17,9},{25,17},{2,26},{10... | collective-permute-start | bytes 1007624 | tf_op jit(solution)/shard_map/ppermute | solution.py:24
  14.5 21.8 %collective-permute-start.8 = (bf16[1312,128]{1,0:T(8,128)(2,1)S(1)}, bf16[1312,128]{1,0:T(8,128)(2,1)S(1)}, u32[]{:S(2)}, u32[]{:S(2)}) collective-permute-start(bf16[1312,128]{1,0:T(8,128)(2,1)S(1)} %get-tuple-element.20), channel_id=1, source_target_pairs={{0,32},{32,64},{64,96},{96,0},{1,33},{33,65},{65,97},{97,1},{2,34}... | collective-permute-start | bytes 1007624 | tf_op jit(solution)/shard_map/ppermute | solution.py:24
  16.1 24.2 %collective-permute-start.7 = (bf16[1312,128]{1,0:T(8,128)(2,1)S(1)}, bf16[1312,128]{1,0:T(8,128)(2,1)S(1)}, u32[]{:S(2)}, u32[]{:S(2)}) collective-permute-start(bf16[1312,128]{1,0:T(8,128)(2,1)S(1)} %get-tuple-element.20), channel_id=1, source_target_pairs={{0,64},{32,96},{64,0},{96,32},{1,65},{33,97},{65,1},{97,33},{2,66}... | collective-permute-start | bytes 1007624 | tf_op jit(solution)/shard_map/ppermute | solution.py:24
  27.4 10.1 %collective-permute-start.6 = (bf16[1312,128]{1,0:T(8,128)(2,1)S(1)}, bf16[1312,128]{1,0:T(8,128)(2,1)S(1)}, u32[]{:S(2)}, u32[]{:S(2)}) collective-permute-start(bf16[1312,128]{1,0:T(8,128)(2,1)S(1)} %get-tuple-element.20), channel_id=1, source_target_pairs={{0,96},{32,0},{64,32},{96,64},{1,97},{33,1},{65,33},{97,65},{2,98}... | collective-permute-start | bytes 1007624 | tf_op jit(solution)/shard_map/ppermute | solution.py:24
  31.3 145.3 %collective-permute-start.22 = (bf16[128,2048]{1,0:T(8,128)(2,1)S(1)}, bf16[128,2048]{1,0:T(8,128)(2,1)S(1)}, u32[]{:S(2)}, u32[]{:S(2)}) collective-permute-start(bf16[128,2048]{1,0:T(8,128)(2,1)S(1)} %get-tuple-element.18.x), channel_id=1, source_target_pairs={{0,2},{2,4},{4,6},{6,0},{1,3},{3,5},{5,7},{7,1},{8,10},{10,12},{12... | collective-permute-start | bytes 1572872 | tf_op jit(solution)/shard_map/ppermute | solution.py:24
  32.7 138.3 %collective-permute-start.20 = (bf16[128,2048]{1,0:T(8,128)(2,1)S(1)}, bf16[128,2048]{1,0:T(8,128)(2,1)S(1)}, u32[]{:S(2)}, u32[]{:S(2)}) collective-permute-start(bf16[128,2048]{1,0:T(8,128)(2,1)S(1)} %get-tuple-element.18.x), channel_id=1, source_target_pairs={{0,4},{2,6},{4,0},{6,2},{1,5},{3,7},{5,1},{7,3},{8,12},{10,14},{12... | collective-permute-start | bytes 1572872 | tf_op jit(solution)/shard_map/ppermute | solution.py:24
  36.3 128.2 %collective-permute-start.18 = (bf16[128,2048]{1,0:T(8,128)(2,1)S(1)}, bf16[128,2048]{1,0:T(8,128)(2,1)S(1)}, u32[]{:S(2)}, u32[]{:S(2)}) collective-permute-start(bf16[128,2048]{1,0:T(8,128)(2,1)S(1)} %get-tuple-element.18.x), channel_id=1, source_target_pairs={{0,6},{2,0},{4,2},{6,4},{1,7},{3,1},{5,3},{7,5},{8,14},{10,8},{12,... | collective-permute-start | bytes 1572872 | tf_op jit(solution)/shard_map/ppermute | solution.py:24
  43.9 19.3 %collective-permute-start.5 = (bf16[4,256,128]{2,1,0:T(8,128)(2,1)S(1)}, bf16[4,256,128]{2,1,0:T(8,128)(2,1)S(1)}, u32[]{:S(2)}, u32[]{:S(2)}) collective-permute-start(bf16[4,256,128]{2,1,0:T(8,128)(2,1)S(1)} %pad_maximum_fusion.2), channel_id=1, source_target_pairs={{0,32},{32,64},{64,96},{96,0},{1,33},{33,65},{65,97},{97,1},{2,34}... | collective-permute-start | bytes 786440 | tf_op jit(solution)/shard_map/ppermute | solution.py:24
  60.6 17.0 %collective-permute-start.10 = (bf16[4,256,128]{2,1,0:T(8,128)(2,1)S(1)}, bf16[4,256,128]{2,1,0:T(8,128)(2,1)S(1)}, u32[]{:S(2)}, u32[]{:S(2)}) collective-permute-start(bf16[4,256,128]{2,1,0:T(8,128)(2,1)S(1)} %pad_maximum_fusion.3), channel_id=1, source_target_pairs={{0,16},{8,24},{16,0},{24,8},{1,17},{9,25},{17,1},{25,9},{2,18},{10... | collective-permute-start | bytes 786440 | tf_op jit(solution)/shard_map/ppermute | solution.py:24
  63.2 12.6 %collective-permute-start.9 = (bf16[4,256,128]{2,1,0:T(8,128)(2,1)S(1)}, bf16[4,256,128]{2,1,0:T(8,128)(2,1)S(1)}, u32[]{:S(2)}, u32[]{:S(2)}) collective-permute-start(bf16[4,256,128]{2,1,0:T(8,128)(2,1)S(1)} %pad_maximum_fusion.3), channel_id=1, source_target_pairs={{0,24},{8,0},{16,8},{24,16},{1,25},{9,1},{17,9},{25,17},{2,26},{10... | collective-permute-start | bytes 786440 | tf_op jit(solution)/shard_map/ppermute | solution.py:24
  77.6 25.8 %collective-permute-start.24 = (bf16[1056,512]{1,0:T(8,128)(2,1)S(1)}, bf16[1056,512]{1,0:T(8,128)(2,1)S(1)}, u32[]{:S(2)}, u32[]{:S(2)}) collective-permute-start(bf16[1056,512]{1,0:T(8,128)(2,1)S(1)} %pad_maximum_fusion), channel_id=1, source_target_pairs={{0,96},{32,0},{64,32},{96,64},{1,97},{33,1},{65,33},{97,65},{2,98}... | collective-permute-start | bytes 3244040 | tf_op jit(solution)/shard_map/ppermute | solution.py:24
  84.7 23.6 %collective-permute-start.31 = (bf16[4,1056,128]{2,1,0:T(8,128)(2,1)S(1)}, bf16[4,1056,128]{2,1,0:T(8,128)(2,1)S(1)}, u32[]{:S(2)}, u32[]{:S(2)}) collective-permute-start(bf16[4,1056,128]{2,1,0:T(8,128)(2,1)S(1)} %pad_maximum_fusion.1), channel_id=1, source_target_pairs={{0,24},{8,0},{16,8},{24,16},{1,25},{9,1},{17,9},{25,17},{2,26},{10... | collective-permute-start | bytes 3244040 | tf_op jit(solution)/shard_map/ppermute | solution.py:24
  103.4 25.8 %collective-permute-start.25 = (bf16[1056,512]{1,0:T(8,128)(2,1)S(1)}, bf16[1056,512]{1,0:T(8,128)(2,1)S(1)}, u32[]{:S(2)}, u32[]{:S(2)}) collective-permute-start(bf16[1056,512]{1,0:T(8,128)(2,1)S(1)} %pad_maximum_fusion), channel_id=1, source_target_pairs={{0,32},{32,64},{64,96},{96,0},{1,33},{33,65},{65,97},{97,1},{2,34}... | collective-permute-start | bytes 3244040 | tf_op jit(solution)/shard_map/ppermute | solution.py:24
  108.4 25.2 %collective-permute-start.32 = (bf16[4,1056,128]{2,1,0:T(8,128)(2,1)S(1)}, bf16[4,1056,128]{2,1,0:T(8,128)(2,1)S(1)}, u32[]{:S(2)}, u32[]{:S(2)}) collective-permute-start(bf16[4,1056,128]{2,1,0:T(8,128)(2,1)S(1)} %pad_maximum_fusion.1), channel_id=1, source_target_pairs={{0,8},{8,16},{16,24},{24,0},{1,9},{9,17},{17,25},{25,1},{2,10},{10... | collective-permute-start | bytes 3244040 | tf_op jit(solution)/shard_map/ppermute | solution.py:24
  129.2 24.5 %collective-permute-start.26 = (bf16[1056,512]{1,0:T(8,128)(2,1)S(1)}, bf16[1056,512]{1,0:T(8,128)(2,1)S(1)}, u32[]{:S(2)}, u32[]{:S(2)}) collective-permute-start(bf16[1056,512]{1,0:T(8,128)(2,1)S(1)} %pad_maximum_fusion), channel_id=1, source_target_pairs={{0,64},{32,96},{64,0},{96,32},{1,65},{33,97},{65,1},{97,33},{2,66}... | collective-permute-start | bytes 3244040 | tf_op jit(solution)/shard_map/ppermute | solution.py:24
  133.6 24.0 %collective-permute-start.33 = (bf16[4,1056,128]{2,1,0:T(8,128)(2,1)S(1)}, bf16[4,1056,128]{2,1,0:T(8,128)(2,1)S(1)}, u32[]{:S(2)}, u32[]{:S(2)}) collective-permute-start(bf16[4,1056,128]{2,1,0:T(8,128)(2,1)S(1)} %pad_maximum_fusion.1), channel_id=1, source_target_pairs={{0,16},{8,24},{16,0},{24,8},{1,17},{9,25},{17,1},{25,9},{2,18},{10... | collective-permute-start | bytes 3244040 | tf_op jit(solution)/shard_map/ppermute | solution.py:24
  164.5 36.2 %collective-permute-start.28 = (bf16[1056,512]{1,0:T(8,128)(2,1)S(1)}, bf16[1056,512]{1,0:T(8,128)(2,1)S(1)}, u32[]{:S(2)}, u32[]{:S(2)}) collective-permute-start(bf16[1056,512]{1,0:T(8,128)(2,1)S(1)} %collective-permute-done.24), channel_id=1, source_target_pairs={{0,1},{1,0},{2,3},{3,2},{4,5},{5,4},{6,7},{7,6},{8,9},{9,8},{10,11... | collective-permute-start | bytes 3244040 | tf_op jit(solution)/shard_map/ppermute | solution.py:24
  165.2 35.5 %collective-permute-start.35 = (bf16[4,1056,128]{2,1,0:T(8,128)(2,1)S(1)}, bf16[4,1056,128]{2,1,0:T(8,128)(2,1)S(1)}, u32[]{:S(2)}, u32[]{:S(2)}) collective-permute-start(bf16[4,1056,128]{2,1,0:T(8,128)(2,1)S(1)} %collective-permute-done.31), channel_id=1, source_target_pairs={{0,1},{1,0},{2,3},{3,2},{4,5},{5,4},{6,7},{7,6},{8,9},{9,8},{10,11... | collective-permute-start | bytes 3244040 | tf_op jit(solution)/shard_map/ppermute | solution.py:24
  169.6 14.5 %collective-permute-start.19 = (bf16[128,2048]{1,0:T(8,128)(2,1)S(1)}, bf16[128,2048]{1,0:T(8,128)(2,1)S(1)}, u32[]{:S(2)}, u32[]{:S(2)}) collective-permute-start(bf16[128,2048]{1,0:T(8,128)(2,1)S(1)} %shard_map.129), channel_id=1, source_target_pairs={{0,2},{2,4},{4,6},{6,0},{1,3},{3,5},{5,7},{7,1},{8,10},{10,12},{12... | collective-permute-start | bytes 1572872 | tf_op jit(solution)/shard_map/ppermute | solution.py:24
  173.8 22.6 %collective-permute-start.21 = (bf16[128,2048]{1,0:T(8,128)(2,1)S(1)}, bf16[128,2048]{1,0:T(8,128)(2,1)S(1)}, u32[]{:S(2)}, u32[]{:S(2)}) collective-permute-start(bf16[128,2048]{1,0:T(8,128)(2,1)S(1)} %shard_map.130), channel_id=1, source_target_pairs={{0,4},{2,6},{4,0},{6,2},{1,5},{3,7},{5,1},{7,3},{8,12},{10,14},{12... | collective-permute-start | bytes 1572872 | tf_op jit(solution)/shard_map/ppermute | solution.py:24
  179.4 19.3 %collective-permute-start.23 = (bf16[128,2048]{1,0:T(8,128)(2,1)S(1)}, bf16[128,2048]{1,0:T(8,128)(2,1)S(1)}, u32[]{:S(2)}, u32[]{:S(2)}) collective-permute-start(bf16[128,2048]{1,0:T(8,128)(2,1)S(1)} %shard_map.131), channel_id=1, source_target_pairs={{0,6},{2,0},{4,2},{6,4},{1,7},{3,1},{5,3},{7,5},{8,14},{10,8},{12,... | collective-permute-start | bytes 1572872 | tf_op jit(solution)/shard_map/ppermute | solution.py:24
  184.1 25.8 %collective-permute-start.37 = (bf16[4,1056,128]{2,1,0:T(8,128)(2,1)S(1)}, bf16[4,1056,128]{2,1,0:T(8,128)(2,1)S(1)}, u32[]{:S(2)}, u32[]{:S(2)}) collective-permute-start(bf16[4,1056,128]{2,1,0:T(8,128)(2,1)S(1)} %collective-permute-done.33), channel_id=1, source_target_pairs={{0,1},{1,0},{2,3},{3,2},{4,5},{5,4},{6,7},{7,6},{8,9},{9,8},{10,11... | collective-permute-start | bytes 3244040 | tf_op jit(solution)/shard_map/ppermute | solution.py:24
  196.5 10.4 %collective-permute-start.36 = (bf16[4,1056,128]{2,1,0:T(8,128)(2,1)S(1)}, bf16[4,1056,128]{2,1,0:T(8,128)(2,1)S(1)}, u32[]{:S(2)}, u32[]{:S(2)}) collective-permute-start(bf16[4,1056,128]{2,1,0:T(8,128)(2,1)S(1)} %collective-permute-done.32), channel_id=1, source_target_pairs={{0,1},{1,0},{2,3},{3,2},{4,5},{5,4},{6,7},{7,6},{8,9},{9,8},{10,11... | collective-permute-start | bytes 3244040 | tf_op jit(solution)/shard_map/ppermute | solution.py:24
  198.7 10.9 %collective-permute-start.30 = (bf16[1056,512]{1,0:T(8,128)(2,1)S(1)}, bf16[1056,512]{1,0:T(8,128)(2,1)S(1)}, u32[]{:S(2)}, u32[]{:S(2)}) collective-permute-start(bf16[1056,512]{1,0:T(8,128)(2,1)S(1)} %collective-permute-done.26), channel_id=1, source_target_pairs={{0,1},{1,0},{2,3},{3,2},{4,5},{5,4},{6,7},{7,6},{8,9},{9,8},{10,11... | collective-permute-start | bytes 3244040 | tf_op jit(solution)/shard_map/ppermute | solution.py:24
  200.8 41.9 %collective-permute-start.43 = (bf16[128,2048]{1,0:T(8,128)(2,1)S(1)}, bf16[128,2048]{1,0:T(8,128)(2,1)S(1)}, u32[]{:S(2)}, u32[]{:S(2)}) collective-permute-start(bf16[128,2048]{1,0:T(8,128)(2,1)S(1)} %get-tuple-element.27.x), channel_id=1, source_target_pairs={{0,2},{2,4},{4,6},{6,0},{1,3},{3,5},{5,7},{7,1},{8,10},{10,12},{12... | collective-permute-start | bytes 1572872 | tf_op jit(solution)/shard_map/ppermute | solution.py:24
  204.0 32.2 %collective-permute-start.41 = (bf16[128,2048]{1,0:T(8,128)(2,1)S(1)}, bf16[128,2048]{1,0:T(8,128)(2,1)S(1)}, u32[]{:S(2)}, u32[]{:S(2)}) collective-permute-start(bf16[128,2048]{1,0:T(8,128)(2,1)S(1)} %get-tuple-element.27.x), channel_id=1, source_target_pairs={{0,4},{2,6},{4,0},{6,2},{1,5},{3,7},{5,1},{7,3},{8,12},{10,14},{12... | collective-permute-start | bytes 1572872 | tf_op jit(solution)/shard_map/ppermute | solution.py:24
  206.9 23.0 %collective-permute-start.39 = (bf16[128,2048]{1,0:T(8,128)(2,1)S(1)}, bf16[128,2048]{1,0:T(8,128)(2,1)S(1)}, u32[]{:S(2)}, u32[]{:S(2)}) collective-permute-start(bf16[128,2048]{1,0:T(8,128)(2,1)S(1)} %get-tuple-element.27.x), channel_id=1, source_target_pairs={{0,6},{2,0},{4,2},{6,4},{1,7},{3,1},{5,3},{7,5},{8,14},{10,8},{12,... | collective-permute-start | bytes 1572872 | tf_op jit(solution)/shard_map/ppermute | solution.py:24
  249.0 14.9 %collective-permute-start.44 = (bf16[128,2048]{1,0:T(8,128)(2,1)S(1)}, bf16[128,2048]{1,0:T(8,128)(2,1)S(1)}, u32[]{:S(2)}, u32[]{:S(2)}) collective-permute-start(bf16[128,2048]{1,0:T(8,128)(2,1)S(1)} %shard_map.141), channel_id=1, source_target_pairs={{0,6},{2,0},{4,2},{6,4},{1,7},{3,1},{5,3},{7,5},{8,14},{10,8},{12,... | collective-permute-start | bytes 1572872 | tf_op jit(solution)/shard_map/ppermute | solution.py:24
  252.2 14.3 %collective-permute-start.42 = (bf16[128,2048]{1,0:T(8,128)(2,1)S(1)}, bf16[128,2048]{1,0:T(8,128)(2,1)S(1)}, u32[]{:S(2)}, u32[]{:S(2)}) collective-permute-start(bf16[128,2048]{1,0:T(8,128)(2,1)S(1)} %shard_map.139), channel_id=1, source_target_pairs={{0,4},{2,6},{4,0},{6,2},{1,5},{3,7},{5,1},{7,3},{8,12},{10,14},{12... | collective-permute-start | bytes 1572872 | tf_op jit(solution)/shard_map/ppermute | solution.py:24
  253.0 25.8 %collective-permute-start.40 = (bf16[128,2048]{1,0:T(8,128)(2,1)S(1)}, bf16[128,2048]{1,0:T(8,128)(2,1)S(1)}, u32[]{:S(2)}, u32[]{:S(2)}) collective-permute-start(bf16[128,2048]{1,0:T(8,128)(2,1)S(1)} %shard_map.137), channel_id=1, source_target_pairs={{0,2},{2,4},{4,6},{6,0},{1,3},{3,5},{5,7},{7,1},{8,10},{10,12},{12... | collective-permute-start | bytes 1572872 | tf_op jit(solution)/shard_map/ppermute | solution.py:24
  (26 other events, 106.2 us)

commit v2 on v1

--- a/solution.py
+++ b/solution.py
@@ -34,16 +34,17 @@
 
 VM = pl.BlockSpec(memory_space=pltpu.VMEM)
 SM = pl.BlockSpec(memory_space=pltpu.SMEM)
-ANY = pl.BlockSpec(memory_space=pl.ANY)
-
-
-def call(body, out, *args, vmem=4, scalars=0, flops=0, scratch=(), where=VM):
+HBM = pl.BlockSpec(memory_space=pltpu.HBM)
+
+
+def call(body, out, *args, vmem=4, scalars=0, flops=0, scratch=(), where=VM, alias=None):
     return pl.pallas_call(
         body,
         in_specs=[SM] * scalars + [where] * (len(args) - scalars),
         out_specs=jax.tree.map(lambda _: VM, out),
         out_shape=out,
         scratch_shapes=scratch,
+        input_output_aliases=alias or {},
         compiler_params=pltpu.CompilerParams(vmem_limit_bytes=vmem * MIB),
         cost_estimate=pl.CostEstimate(flops=flops, transcendentals=0, bytes_accessed=0),
     )(*args)
@@ -127,11 +128,14 @@
     return jnp.where(v > -0.5, -v * series, 1.0 - exp_v)
 
 
-def mix_body(x, in_own, in_par, taps, gates, rate, out_own, out_par, out, proj, states):
-    rows = lax.broadcasted_iota(jnp.int32, (SEQ, BLK), 0)
+def mix_body(
+    x0, x1, in_own, in_par, taps, gates, rate, out_own, out_par, out0, out1, proj, states
+):
+    rows = lax.broadcasted_iota(jnp.int32, (2 * SEQ, BLK), 0) % SEQ
+    x = jnp.concatenate([x0[...], x1[...]], axis=0)
     for half, w in enumerate((in_own, in_par)):
         proj[:, half * 256 : (half + 1) * 256] = jnp.dot(
-            x[...], w[...], preferred_element_type=F32
+            x, w[...], preferred_element_type=F32
         ).astype(BF16)
 
     def tile(t, carry):
@@ -161,7 +165,9 @@
         cols = pl.ds(pl.multiple_of(n * 512, 512), 512)
         part = jnp.dot(states[:, :256], out_own[:, cols], preferred_element_type=F32)
         part = part + jnp.dot(states[:, 256:], out_par[:, cols], preferred_element_type=F32)
-        out[:, cols] = part.astype(BF16)
+        part = part.astype(BF16)
+        out0[:, cols] = part[:SEQ]
+        out1[:, cols] = part[SEQ:]
         return carry
 
     lax.fori_loop(0, 4, column, 0)
@@ -171,17 +177,55 @@
     return lax.dot_general(a, b, (((1,), (1,)), ((), ())), preferred_element_type=F32)
 
 
-def tick_body(taps, out):
-    out[...] = taps[...]
-
-
-def up_body(x, gate, val, taps, out, buf):
-    rows = lax.broadcasted_iota(jnp.int32, (SEQ, BLK), 0)
+ROWS = 32
+
+
+def put_pieces(ks, pieces, gate, val, down):
+    for n, k in enumerate(ks):
+        for c in range(2):
+            a, b = pieces[4 * n + 2 * c], pieces[4 * n + 2 * c + 1]
+            top = c * HID
+            lanes = slice(k * 512, (k + 1) * 512)
+
+            def up_rows(r, carry):
+                src = pl.ds(pl.multiple_of(r * ROWS, ROWS), ROWS)
+                dst = pl.ds(pl.multiple_of(top + r * ROWS, ROWS), ROWS)
+                gate[dst, lanes] = a[src]
+                for i in range(4):
+                    at = (4 * i + k) * BLK
+                    val[dst, at : at + BLK] = b[i, src]
+                return carry
+
+            def down_rows(r, carry):
+                src = pl.ds(pl.multiple_of(HID + r * ROWS, ROWS), ROWS)
+                dst = pl.ds(pl.multiple_of(top + r * ROWS, ROWS), ROWS)
+                low = pl.ds(pl.multiple_of(top + HID // 2 + r * ROWS, ROWS), ROWS)
+                down[dst, lanes] = a[src]
+                for i in range(4):
+                    at = (4 * i + k) * BLK
+                    down[low, at : at + BLK] = b[i, src]
+                return carry
+
+            lax.fori_loop(0, HID // ROWS, up_rows, 0)
+            lax.fori_loop(0, HID // 2 // ROWS, down_rows, 0)
+
+
+def early_body(*refs):
+    put_pieces((0, 1, 3), refs[:12], *refs[12:])
+
+
+def late_body(*refs):
+    put_pieces((2,), refs[:4], *refs[7:])
+
+
+def up_body(x0, x1, gate, val, taps, out, buf):
+    rows = lax.broadcasted_iota(jnp.int32, (2 * SEQ, BLK), 0) % SEQ
     last = 2 * HID // BLK - 1
 
     def product(t):
         cols = pl.ds(pl.multiple_of(t * BLK, BLK), BLK)
-        return nt_dot(x[...], jnp.concatenate([gate[cols], val[cols]], axis=0))
+        x = jnp.concatenate([x0[...], x1[...]], axis=0)
+        return nt_dot(x, jnp.concatenate([gate[cols], val[cols]], axis=0))
 
     def finish(t, both):
         cols = pl.ds(pl.multiple_of(t * BLK, BLK), BLK)
@@ -192,25 +236,27 @@
             conv = conv + delayed(g, 2 - k, rows, 0.0) * taps[k : k + 1, cols]
         out[:, cols] = (conv * sigmoid(conv) * v).astype(BF16)
 
-    buf[0] = product(0)
+    buf[...] = product(0)
 
     def tile(i, carry):
         t = 2 * i
         one = product(t + 1)
-        finish(t, buf[0])
+        finish(t, buf[...])
         two = product(t + 2)
         finish(t + 1, one)
-        buf[0] = two
+        buf[...] = two
         return carry
 
     lax.fori_loop(0, last // 2, tile, 0)
-    finish(last, buf[0])
-
-
-def down_body(h, down, out):
+    finish(last, buf[...])
+
+
+def down_body(h, down, out0, out1):
     def tile(n, carry):
         cols = pl.ds(pl.multiple_of(n * 512, 512), 512)
-        out[:, cols] = jnp.dot(h[...], down[:, cols], preferred_element_type=F32).astype(BF16)
+        part = jnp.dot(h[...], down[:, cols], preferred_element_type=F32).astype(BF16)
+        out0[:, cols] = part[:SEQ]
+        out1[:, cols] = part[SEQ:]
         return carry
 
     lax.fori_loop(0, 4, tile, 0)
@@ -260,7 +306,7 @@
         up_val_w.T,
         down_weight,
         scalars=1,
-        where=ANY,
+        where=HBM,
         scratch=[
             pltpu.VMEM((SEQ, D), BF16),
             pltpu.VMEM((1, D), F32),
@@ -316,25 +362,13 @@
 
     ua_par = [partner(v) for v in ua]
     ub_par = [partner(v) for v in ub]
-    gate, val, down = [], [], []
-    for c, (wa, wb) in enumerate(((ua, ub), (ua_par, ub_par))):
-        top = c * HID
-        for k in (0, 1, 3, 2):
-            gate.append((wa[k][:HID], top, k * 512))
-            down.append((wa[k][HID:], top, k * 512))
-            for i in range(4):
-                at = (4 * i + k) * BLK
-                val.append((wb[k][i, :HID], top, at))
-                down.append((wb[k][i, HID:], top + HID // 2, at))
-    gate = placed((2 * HID, D), gate)
-    val = placed((2 * HID, D), val)
-    down = placed((2 * HID, D), down)
 
     parts = [None] * 4
-    for j in (1, 3, 2, 0):
-        part = call(
+    for i, j in ((1, 3), (2, 0)):
+        pair = call(
             mix_body,
-            sds((SEQ, D)),
+            [sds((SEQ, D))] * 2,
+            rows1[i],
             rows1[j],
             in_own,
             in_par,
@@ -343,28 +377,42 @@
             rate,
             out_own,
             out_par,
-            flops=2 * SEQ * D * 512 * 2,
-            scratch=[pltpu.VMEM((SEQ, 512), BF16)] * 2,
+            flops=2 * 2 * SEQ * D * 512 * 2,
+            scratch=[pltpu.VMEM((2 * SEQ, 512), BF16)] * 2,
         )
-        parts[j] = sums_sent(part, j) if j else part
+        for k, part in zip((i, j), pair):
+            parts[k] = sums_sent(part, k) if k else part
     middle, normed_two = call(
         second_norm_body, [sds((SEQ, D)), sds((SEQ, D))], resid_rel, *parts, gain2
     )
     rows2 = fetch_all(normed_two, "y")
-    ftaps = call(tick_body, sds((3, 2 * HID), F32), ftaps)
-    for j in (0, 1, 3, 2):
+
+    whole = [sds((2 * HID, D))] * 3
+
+    def pieces(*ks):
+        return [v[k] for k in ks for v in (ua, ub, ua_par, ub_par)]
+
+    weights = call(early_body, whole, *pieces(0, 1, 3))
+    weights = call(late_body, whole, *pieces(2), *weights, alias={4: 0, 5: 1, 6: 2})
+    gate, val, down = weights
+
+    for i, j in ((1, 3), (2, 0)):
         hidden = call(
             up_body,
-            sds((SEQ, 2 * HID)),
+            sds((2 * SEQ, 2 * HID)),
+            rows2[i],
             rows2[j],
             gate,
             val,
             ftaps,
-            flops=2 * SEQ * D * 1408 * 2,
-            scratch=[pltpu.VMEM((1, SEQ, 256), F32)],
+            flops=2 * 2 * SEQ * D * 1408 * 2,
+            scratch=[pltpu.VMEM((2 * SEQ, 256), F32)],
         )
-        part = call(down_body, sds((SEQ, D)), hidden, down, flops=2 * SEQ * D * 1408)
-        parts[j] = sums_sent(part, j) if j else part
+        pair = call(
+            down_body, [sds((SEQ, D))] * 2, hidden, down, flops=2 * 2 * SEQ * D * 1408
+        )
+        for k, part in zip((i, j), pair):
+            parts[k] = sums_sent(part, k) if k else part
     return call(last_sum_body, sds((SEQ, D)), order, middle, *parts, scalars=1)
 
 

time: 281 us -> 222 us (0.79)
  waiting for transfers between devices: 154 us -> 115 us
  Pallas kernels: 41.2 us -> 30.1 us
  local copies, waits for them, and re-layouts: 13.7 us -> 7.93 us
    ppermute x45, waiting for transfers between devices: 154 us -> 115 us  [fetch(): return lax.ppermute(a, axis, [(i, (i - ahead) % size) for i in range(size)])]
    pallas_call x16 -> x11, Pallas kernels: 41.2 us -> 30.1 us  [call(): pl.pallas_call(body, in_specs=[SM] * scalars + [where] * (len(args) - sca...]
    dynamic_update_slice x113 -> x33, local copies, waits for them, and re-layouts: 6.45 us -> 0.78 us  [placed(): out = lax.dynamic_update_slice(out, piece, (r, c))]
  transfers between devices with their start and end apart: 45 -> 45, of which waited for: 25 -> 20; matrix products, arithmetic and copies ran while one was open for 3% -> 1% of each run, Pallas kernels for 11% -> 9%
where the time goes in v2:
time: 222 us; the launch traced here: 221 us
  waiting for transfers between devices  115 us (52%)
  starting transfers between devices  67.6 us (30%)
  Pallas kernels  30.1 us (14%)
  local copies, waits for them, and re-layouts  7.93 us (4%)
    ppermute x45, waiting for transfers between devices, fetch(): return lax.ppermute(a, axis, [(i, (i - ahead) % size) for i in range(size)])  115 us
    ppermute x45, starting transfers between devices, fetch(): return lax.ppermute(a, axis, [(i, (i - ahead) % size) for i in range(size)])  67.6 us
    pallas_call x11, Pallas kernels, call(): pl.pallas_call(body, in_specs=[SM] * scalars + [where] * (len(args) - sca...  30.1 us
    unnamed x28, local copies, waits for them, and re-layouts  6.9 us
  transfers between devices with their start and end apart: 45, of which 20 were waited for; matrix products, arithmetic and copies ran while one was open for 1% of the time, Pallas kernels for 9%

profile of v2, /device:TPU:1, one launch (start us, length us, event | category | flops | bytes accessed | tf_op | source)
XLA Modules:
  0.0 221.5 jit_solution(3490259551202704024)
XLA Ops:
  8.8 3.4 %collective-permute-start.1 = (bf16[1312,128]{1,0:T(8,128)(2,1)S(1)}, bf16[1312,128]{1,0:T(8,128)(2,1)S(1)}, u32[]{:S(2)}, u32[]{:S(2)}) collective-permute-start(bf16[1312,128]{1,0:T(8,128)(2,1)S(1)} %get-tuple-element.33), channel_id=1, source_target_pairs={{0,24},{8,0},{16,8},{24,16},{1,25},{9,1},{17,9},{25,17},{2,26},{10... | collective-permute-start | bytes 1007624 | tf_op jit(solution)/shard_map/ppermute | solution.py:24
  14.9 3.3 %collective-permute-start.8 = (bf16[1312,128]{1,0:T(8,128)(2,1)S(1)}, bf16[1312,128]{1,0:T(8,128)(2,1)S(1)}, u32[]{:S(2)}, u32[]{:S(2)}) collective-permute-start(bf16[1312,128]{1,0:T(8,128)(2,1)S(1)} %get-tuple-element.34), channel_id=1, source_target_pairs={{0,64},{32,96},{64,0},{96,32},{1,65},{33,97},{65,1},{97,33},{2,66}... | collective-permute-start | bytes 1007624 | tf_op jit(solution)/shard_map/ppermute | solution.py:24
  19.9 3.4 %collective-permute-start.7 = (bf16[1312,128]{1,0:T(8,128)(2,1)S(1)}, bf16[1312,128]{1,0:T(8,128)(2,1)S(1)}, u32[]{:S(2)}, u32[]{:S(2)}) collective-permute-start(bf16[1312,128]{1,0:T(8,128)(2,1)S(1)} %get-tuple-element.34), channel_id=1, source_target_pairs={{0,96},{32,0},{64,32},{96,64},{1,97},{33,1},{65,33},{97,65},{2,98}... | collective-permute-start | bytes 1007624 | tf_op jit(solution)/shard_map/ppermute | solution.py:24
  23.3 3.0 %collective-permute-start = (bf16[128,2048]{1,0:T(8,128)(2,1)S(1)}, bf16[128,2048]{1,0:T(8,128)(2,1)S(1)}, u32[]{:S(2)}, u32[]{:S(2)}) collective-permute-start(bf16[128,2048]{1,0:T(8,128)(2,1)S(1)} %get-tuple-element.32.x1), channel_id=1, source_target_pairs={{0,4},{2,6},{4,0},{6,2},{1,5},{3,7},{5,1},{7,3},{8,12},{10,14},{12... | collective-permute-start | bytes 1572872 | tf_op jit(solution)/shard_map/ppermute | solution.py:24
  26.3 4.4 %collective-permute-done.3 = bf16[1312,128]{1,0:T(8,128)(2,1)S(1)} collective-permute-done((bf16[1312,128]{1,0:T(8,128)(2,1)S(1)}, bf16[1312,128]{1,0:T(8,128)(2,1)S(1)}, u32[]{:S(2)}, u32[]{:S(2)}) %collective-permute-start.3) | collective-permute-done | bytes 335904 | tf_op jit(solution)/shard_map/ppermute | solution.py:24
  30.7 2.7 %collective-permute-start.19 = (bf16[128,2048]{1,0:T(8,128)(2,1)S(1)}, bf16[128,2048]{1,0:T(8,128)(2,1)S(1)}, u32[]{:S(2)}, u32[]{:S(2)}) collective-permute-start(bf16[128,2048]{1,0:T(8,128)(2,1)S(1)} %get-tuple-element.32.x1), channel_id=1, source_target_pairs={{0,6},{2,0},{4,2},{6,4},{1,7},{3,1},{5,3},{7,5},{8,14},{10,8},{12,... | collective-permute-start | bytes 1572872 | tf_op jit(solution)/shard_map/ppermute | solution.py:24
  33.5 3.8 %collective-permute-start.4 = (bf16[4,256,128]{2,1,0:T(8,128)(2,1)S(1)}, bf16[4,256,128]{2,1,0:T(8,128)(2,1)S(1)}, u32[]{:S(2)}, u32[]{:S(2)}) collective-permute-start(bf16[4,256,128]{2,1,0:T(8,128)(2,1)S(1)} %pad_maximum_fusion.2), channel_id=1, source_target_pairs={{0,96},{32,0},{64,32},{96,64},{1,97},{33,1},{65,33},{97,65},{2,98}... | collective-permute-start | bytes 786440 | tf_op jit(solution)/shard_map/ppermute | solution.py:24
  38.8 9.3 %collective-permute-done.4 = bf16[4,256,128]{2,1,0:T(8,128)(2,1)S(1)} collective-permute-done((bf16[4,256,128]{2,1,0:T(8,128)(2,1)S(1)}, bf16[4,256,128]{2,1,0:T(8,128)(2,1)S(1)}, u32[]{:S(2)}, u32[]{:S(2)}) %collective-permute-start.4) | collective-permute-done | bytes 262176 | tf_op jit(solution)/shard_map/ppermute | solution.py:24
  48.5 3.9 %collective-permute-done.6 = bf16[4,256,128]{2,1,0:T(8,128)(2,1)S(1)} collective-permute-done((bf16[4,256,128]{2,1,0:T(8,128)(2,1)S(1)}, bf16[4,256,128]{2,1,0:T(8,128)(2,1)S(1)}, u32[]{:S(2)}, u32[]{:S(2)}) %collective-permute-start.6) | collective-permute-done | bytes 262176 | tf_op jit(solution)/shard_map/ppermute | solution.py:24
  54.4 7.8 %collective-permute-start.14 = (f32[4,256]{1,0:T(4,128)S(1)}, f32[4,256]{1,0:T(4,128)S(1)}, u32[]{:S(2)}, u32[]{:S(2)}) collective-permute-start(f32[4,256]{1,0:T(4,128)S(1)} %copy-done.11), channel_id=1, source_target_pairs={{0,1},{1,0},{2,3},{3,2},{4,5},{5,4},{6,7},{7,6},{8,9},{9,8},{10,11... | collective-permute-start | bytes 12296 | tf_op jit(solution)/shard_map/ppermute | solution.py:24
  69.2 5.7 %collective-permute-start.31 = (bf16[1056,512]{1,0:T(8,128)(2,1)S(1)}, bf16[1056,512]{1,0:T(8,128)(2,1)S(1)}, u32[]{:S(2)}, u32[]{:S(2)}) collective-permute-start(bf16[1056,512]{1,0:T(8,128)(2,1)S(1)} %pad_maximum_fusion.refs_0_), channel_id=1, source_target_pairs={{0,96},{32,0},{64,32},{96,64},{1,97},{33,1},{65,33},{97,65},{2,98}... | collective-permute-start | bytes 3244040 | tf_op jit(solution)/shard_map/ppermute | solution.py:24
  74.9 6.9 %collective-permute-done.20.x1 = bf16[128,2048]{1,0:T(8,128)(2,1)S(1)} collective-permute-done((bf16[128,2048]{1,0:T(8,128)(2,1)S(1)}, bf16[128,2048]{1,0:T(8,128)(2,1)S(1)}, u32[]{:S(2)}, u32[]{:S(2)}) %collective-permute-start.20) | collective-permute-done | bytes 524320 | tf_op jit(solution)/shard_map/ppermute | solution.py:24
  83.0 9.6 %collective-permute-done.25.refs_0_ = bf16[1056,512]{1,0:T(8,128)(2,1)S(1)} collective-permute-done((bf16[1056,512]{1,0:T(8,128)(2,1)S(1)}, bf16[1056,512]{1,0:T(8,128)(2,1)S(1)}, u32[]{:S(2)}, u32[]{:S(2)}) %collective-permute-start.25) | collective-permute-done | bytes 1081376 | tf_op jit(solution)/shard_map/ppermute | solution.py:24
  99.0 18.7 %collective-permute-done.31.refs_4_ = bf16[1056,512]{1,0:T(8,128)(2,1)S(1)} collective-permute-done((bf16[1056,512]{1,0:T(8,128)(2,1)S(1)}, bf16[1056,512]{1,0:T(8,128)(2,1)S(1)}, u32[]{:S(2)}, u32[]{:S(2)}) %collective-permute-start.31) | collective-permute-done | bytes 1081376 | tf_op jit(solution)/shard_map/ppermute | solution.py:24
  119.4 4.2 %shard_map.128 = (bf16[128,2048]{1,0:T(8,128)(2,1)S(1)}, bf16[128,2048]{1,0:T(8,128)(2,1)S(1)}) custom-call(bf16[128,2048]{1,0:T(8,128)(2,1)S(1)} %collective-permute-done.x0, bf16[128,2048]{1,0:T(8,128)(2,1)S(1)} %get-tuple-element.32.x1, bf16[2048,256]{1,0:T(8,128)(2,1)S(1)} %get-tuple-element.58.in_own, ...), custom_call_target="tpu_custom_call" | custom-call | flops 1073741824 | tf_op jit(solution)/shard_map/pallas_call | solution.py:41
  123.7 4.2 %shard_map.129 = (bf16[128,2048]{1,0:T(8,128)(2,1)S(1)}, bf16[128,2048]{1,0:T(8,128)(2,1)S(1)}) custom-call(bf16[128,2048]{1,0:T(8,128)(2,1)S(1)} %collective-permute-done.19.x0, bf16[128,2048]{1,0:T(8,128)(2,1)S(1)} %collective-permute-done.20.x1, bf16[2048,256]{1,0:T(8,128)(2,1)S(1)} %get-tuple-element.58.in_own, ...), custom_call_target="tpu_custom_call" | custom-call | flops 1073741824 | tf_op jit(solution)/shard_map/pallas_call | solution.py:41
  129.3 2.6 %collective-permute-start.22 = (bf16[128,2048]{1,0:T(8,128)(2,1)S(1)}, bf16[128,2048]{1,0:T(8,128)(2,1)S(1)}, u32[]{:S(2)}, u32[]{:S(2)}) collective-permute-start(bf16[128,2048]{1,0:T(8,128)(2,1)S(1)} %get-tuple-element.41), channel_id=1, source_target_pairs={{0,4},{2,6},{4,0},{6,2},{1,5},{3,7},{5,1},{7,3},{8,12},{10,14},{12... | collective-permute-start | bytes 1572872 | tf_op jit(solution)/shard_map/ppermute | solution.py:24
  131.9 11.9 %collective-permute-done.35.refs_8_ = bf16[1056,512]{1,0:T(8,128)(2,1)S(1)} collective-permute-done((bf16[1056,512]{1,0:T(8,128)(2,1)S(1)}, bf16[1056,512]{1,0:T(8,128)(2,1)S(1)}, u32[]{:S(2)}, u32[]{:S(2)}) %collective-permute-start.35) | collective-permute-done | bytes 1081376 | tf_op jit(solution)/shard_map/ppermute | solution.py:24
  143.9 2.7 %collective-permute-start.23 = (bf16[128,2048]{1,0:T(8,128)(2,1)S(1)}, bf16[128,2048]{1,0:T(8,128)(2,1)S(1)}, u32[]{:S(2)}, u32[]{:S(2)}) collective-permute-start(bf16[128,2048]{1,0:T(8,128)(2,1)S(1)} %get-tuple-element.42), channel_id=1, source_target_pairs={{0,6},{2,0},{4,2},{6,4},{1,7},{3,1},{5,3},{7,5},{8,14},{10,8},{12,... | collective-permute-start | bytes 1572872 | tf_op jit(solution)/shard_map/ppermute | solution.py:24
  148.6 6.5 %collective-permute-done.22.p2 = bf16[128,2048]{1,0:T(8,128)(2,1)S(1)} collective-permute-done((bf16[128,2048]{1,0:T(8,128)(2,1)S(1)}, bf16[128,2048]{1,0:T(8,128)(2,1)S(1)}, u32[]{:S(2)}, u32[]{:S(2)}) %collective-permute-start.22) | collective-permute-done | bytes 524320 | tf_op jit(solution)/shard_map/ppermute | solution.py:24
  156.2 2.5 %collective-permute-start.27 = (bf16[1056,512]{1,0:T(8,128)(2,1)S(1)}, bf16[1056,512]{1,0:T(8,128)(2,1)S(1)}, u32[]{:S(2)}, u32[]{:S(2)}) collective-permute-start(bf16[1056,512]{1,0:T(8,128)(2,1)S(1)} %collective-permute-done.25.refs_0_), channel_id=1, source_target_pairs={{0,1},{1,0},{2,3},{3,2},{4,5},{5,4},{6,7},{7,6},{8,9},{9,8},{10,11... | collective-permute-start | bytes 3244040 | tf_op jit(solution)/shard_map/ppermute | solution.py:24
  159.3 2.5 %collective-permute-start.24 = (bf16[128,2048]{1,0:T(8,128)(2,1)S(1)}, bf16[128,2048]{1,0:T(8,128)(2,1)S(1)}, u32[]{:S(2)}, u32[]{:S(2)}) collective-permute-start(bf16[128,2048]{1,0:T(8,128)(2,1)S(1)} %get-tuple-element.45.x1), channel_id=1, source_target_pairs={{0,4},{2,6},{4,0},{6,2},{1,5},{3,7},{5,1},{7,3},{8,12},{10,14},{12... | collective-permute-start | bytes 1572872 | tf_op jit(solution)/shard_map/ppermute | solution.py:24
  163.5 2.7 %shard_map.131 = (bf16[1408,2048]{1,0:T(8,128)(2,1)S(1)}, bf16[1408,2048]{1,0:T(8,128)(2,1)S(1)}, bf16[1408,2048]{1,0:T(8,128)(2,1)S(1)}) custom-call(bf16[1056,512]{1,0:T(8,128)(2,1)S(1)} %pad_maximum_fusion.refs_0_, bf16[4,1056,128]{2,1,0:T(8,128)(2,1)S(1)} %pad_maximum_fusion.1.refs_1_, bf16[1056,512]{1,0:T(8,128)(2,1)S(1)} %collective-permute-done.29.refs_2_, ...), custom_call_target="tpu_custom_call" | custom-call | tf_op jit(solution)/shard_map/pallas_call | solution.py:41
  167.2 6.7 %collective-permute-done.24.x0 = bf16[128,2048]{1,0:T(8,128)(2,1)S(1)} collective-permute-done((bf16[128,2048]{1,0:T(8,128)(2,1)S(1)}, bf16[128,2048]{1,0:T(8,128)(2,1)S(1)}, u32[]{:S(2)}, u32[]{:S(2)}) %collective-permute-start.24) | collective-permute-done | bytes 524320 | tf_op jit(solution)/shard_map/ppermute | solution.py:24
  173.9 4.6 %shard_map.133.h = bf16[256,1408]{1,0:T(8,128)(2,1)S(1)} custom-call(bf16[128,2048]{1,0:T(8,128)(2,1)S(1)} %collective-permute-done.24.x0, bf16[128,2048]{1,0:T(8,128)(2,1)S(1)} %get-tuple-element.45.x1, bf16[1408,2048]{1,0:T(8,128)(2,1)S(1)} %get-tuple-element.49.gate, bf16[1408,2048]{1,0:T(8,128)(2,1)S(1)} %get-tuple-element.50.val, ...), custom_call_target="tpu_custom_call" | custom-call | flops 2952790016 | tf_op jit(solution)/shard_map/pallas_call | solution.py:41
  178.5 2.3 %shard_map.134 = (bf16[128,2048]{1,0:T(8,128)(2,1)S(1)}, bf16[128,2048]{1,0:T(8,128)(2,1)S(1)}) custom-call(bf16[256,1408]{1,0:T(8,128)(2,1)S(1)} %shard_map.133.h, bf16[1408,2048]{1,0:T(8,128)(2,1)S(1)} %get-tuple-element.52.down), custom_call_target="tpu_custom_call" | custom-call | flops 1476395008 | tf_op jit(solution)/shard_map/pallas_call | solution.py:41
  180.8 5.3 %collective-permute-done.40.x0 = bf16[128,2048]{1,0:T(8,128)(2,1)S(1)} collective-permute-done((bf16[128,2048]{1,0:T(8,128)(2,1)S(1)}, bf16[128,2048]{1,0:T(8,128)(2,1)S(1)}, u32[]{:S(2)}, u32[]{:S(2)}) %collective-permute-start.40) | collective-permute-done | bytes 524320 | tf_op jit(solution)/shard_map/ppermute | solution.py:24
  186.1 4.6 %shard_map.135.h = bf16[256,1408]{1,0:T(8,128)(2,1)S(1)} custom-call(bf16[128,2048]{1,0:T(8,128)(2,1)S(1)} %collective-permute-done.40.x0, bf16[128,2048]{1,0:T(8,128)(2,1)S(1)} %collective-permute-done.41.x1, bf16[1408,2048]{1,0:T(8,128)(2,1)S(1)} %get-tuple-element.49.gate, bf16[1408,2048]{1,0:T(8,128)(2,1)S(1)} %get-tuple-element.50.val, ...), custom_call_target="tpu_custom_call" | custom-call | flops 2952790016 | tf_op jit(solution)/shard_map/pallas_call | solution.py:41
  190.8 2.3 %shard_map.136 = (bf16[128,2048]{1,0:T(8,128)(2,1)S(1)}, bf16[128,2048]{1,0:T(8,128)(2,1)S(1)}) custom-call(bf16[256,1408]{1,0:T(8,128)(2,1)S(1)} %shard_map.135.h, bf16[1408,2048]{1,0:T(8,128)(2,1)S(1)} %get-tuple-element.52.down), custom_call_target="tpu_custom_call" | custom-call | flops 1476395008 | tf_op jit(solution)/shard_map/pallas_call | solution.py:41
  194.0 3.2 %collective-permute-start.43 = (bf16[128,2048]{1,0:T(8,128)(2,1)S(1)}, bf16[128,2048]{1,0:T(8,128)(2,1)S(1)}, u32[]{:S(2)}, u32[]{:S(2)}) collective-permute-start(bf16[128,2048]{1,0:T(8,128)(2,1)S(1)} %get-tuple-element.55), channel_id=1, source_target_pairs={{0,4},{2,6},{4,0},{6,2},{1,5},{3,7},{5,1},{7,3},{8,12},{10,14},{12... | collective-permute-start | bytes 1572872 | tf_op jit(solution)/shard_map/ppermute | solution.py:24
  197.4 9.4 %collective-permute-done.42.p1 = bf16[128,2048]{1,0:T(8,128)(2,1)S(1)} collective-permute-done((bf16[128,2048]{1,0:T(8,128)(2,1)S(1)}, bf16[128,2048]{1,0:T(8,128)(2,1)S(1)}, u32[]{:S(2)}, u32[]{:S(2)}) %collective-permute-start.42) | collective-permute-done | bytes 524320 | tf_op jit(solution)/shard_map/ppermute | solution.py:24
  206.8 12.9 %collective-permute-done.43.p2 = bf16[128,2048]{1,0:T(8,128)(2,1)S(1)} collective-permute-done((bf16[128,2048]{1,0:T(8,128)(2,1)S(1)}, bf16[128,2048]{1,0:T(8,128)(2,1)S(1)}, u32[]{:S(2)}, u32[]{:S(2)}) %collective-permute-start.43) | collective-permute-done | bytes 524320 | tf_op jit(solution)/shard_map/ppermute | solution.py:24
  (161 shorter events, 43.7 us)
Async XLA Ops:
  12.7 18.0 %collective-permute-start.3 = (bf16[1312,128]{1,0:T(8,128)(2,1)S(1)}, bf16[1312,128]{1,0:T(8,128)(2,1)S(1)}, u32[]{:S(2)}, u32[]{:S(2)}) collective-permute-start(bf16[1312,128]{1,0:T(8,128)(2,1)S(1)} %get-tuple-element.33), channel_id=1, source_target_pairs={{0,8},{8,16},{16,24},{24,0},{1,9},{9,17},{17,25},{25,1},{2,10},{10... | collective-permute-start | bytes 1007624 | tf_op jit(solution)/shard_map/ppermute | solution.py:24
  13.3 20.2 %collective-permute-start.9 = (bf16[1312,128]{1,0:T(8,128)(2,1)S(1)}, bf16[1312,128]{1,0:T(8,128)(2,1)S(1)}, u32[]{:S(2)}, u32[]{:S(2)}) collective-permute-start(bf16[1312,128]{1,0:T(8,128)(2,1)S(1)} %get-tuple-element.34), channel_id=1, source_target_pairs={{0,32},{32,64},{64,96},{96,0},{1,33},{33,65},{65,97},{97,1},{2,34}... | collective-permute-start | bytes 1007624 | tf_op jit(solution)/shard_map/ppermute | solution.py:24
  14.9 22.4 %collective-permute-start.8 = (bf16[1312,128]{1,0:T(8,128)(2,1)S(1)}, bf16[1312,128]{1,0:T(8,128)(2,1)S(1)}, u32[]{:S(2)}, u32[]{:S(2)}) collective-permute-start(bf16[1312,128]{1,0:T(8,128)(2,1)S(1)} %get-tuple-element.34), channel_id=1, source_target_pairs={{0,64},{32,96},{64,0},{96,32},{1,65},{33,97},{65,1},{97,33},{2,66}... | collective-permute-start | bytes 1007624 | tf_op jit(solution)/shard_map/ppermute | solution.py:24
  19.9 17.6 %collective-permute-start.7 = (bf16[1312,128]{1,0:T(8,128)(2,1)S(1)}, bf16[1312,128]{1,0:T(8,128)(2,1)S(1)}, u32[]{:S(2)}, u32[]{:S(2)}) collective-permute-start(bf16[1312,128]{1,0:T(8,128)(2,1)S(1)} %get-tuple-element.34), channel_id=1, source_target_pairs={{0,96},{32,0},{64,32},{96,64},{1,97},{33,1},{65,33},{97,65},{2,98}... | collective-permute-start | bytes 1007624 | tf_op jit(solution)/shard_map/ppermute | solution.py:24
  23.3 45.9 %collective-permute-start = (bf16[128,2048]{1,0:T(8,128)(2,1)S(1)}, bf16[128,2048]{1,0:T(8,128)(2,1)S(1)}, u32[]{:S(2)}, u32[]{:S(2)}) collective-permute-start(bf16[128,2048]{1,0:T(8,128)(2,1)S(1)} %get-tuple-element.32.x1), channel_id=1, source_target_pairs={{0,4},{2,6},{4,0},{6,2},{1,5},{3,7},{5,1},{7,3},{8,12},{10,14},{12... | collective-permute-start | bytes 1572872 | tf_op jit(solution)/shard_map/ppermute | solution.py:24
  30.7 38.5 %collective-permute-start.19 = (bf16[128,2048]{1,0:T(8,128)(2,1)S(1)}, bf16[128,2048]{1,0:T(8,128)(2,1)S(1)}, u32[]{:S(2)}, u32[]{:S(2)}) collective-permute-start(bf16[128,2048]{1,0:T(8,128)(2,1)S(1)} %get-tuple-element.32.x1), channel_id=1, source_target_pairs={{0,6},{2,0},{4,2},{6,4},{1,7},{3,1},{5,3},{7,5},{8,14},{10,8},{12,... | collective-permute-start | bytes 1572872 | tf_op jit(solution)/shard_map/ppermute | solution.py:24
  33.5 14.5 %collective-permute-start.4 = (bf16[4,256,128]{2,1,0:T(8,128)(2,1)S(1)}, bf16[4,256,128]{2,1,0:T(8,128)(2,1)S(1)}, u32[]{:S(2)}, u32[]{:S(2)}) collective-permute-start(bf16[4,256,128]{2,1,0:T(8,128)(2,1)S(1)} %pad_maximum_fusion.2), channel_id=1, source_target_pairs={{0,96},{32,0},{64,32},{96,64},{1,97},{33,1},{65,33},{97,65},{2,98}... | collective-permute-start | bytes 786440 | tf_op jit(solution)/shard_map/ppermute | solution.py:24
  37.5 14.9 %collective-permute-start.6 = (bf16[4,256,128]{2,1,0:T(8,128)(2,1)S(1)}, bf16[4,256,128]{2,1,0:T(8,128)(2,1)S(1)}, u32[]{:S(2)}, u32[]{:S(2)}) collective-permute-start(bf16[4,256,128]{2,1,0:T(8,128)(2,1)S(1)} %pad_maximum_fusion.2), channel_id=1, source_target_pairs={{0,32},{32,64},{64,96},{96,0},{1,33},{33,65},{65,97},{97,1},{2,34}... | collective-permute-start | bytes 786440 | tf_op jit(solution)/shard_map/ppermute | solution.py:24
  48.1 14.2 %collective-permute-start.11 = (bf16[4,256,128]{2,1,0:T(8,128)(2,1)S(1)}, bf16[4,256,128]{2,1,0:T(8,128)(2,1)S(1)}, u32[]{:S(2)}, u32[]{:S(2)}) collective-permute-start(bf16[4,256,128]{2,1,0:T(8,128)(2,1)S(1)} %pad_maximum_fusion.3), channel_id=1, source_target_pairs={{0,16},{8,24},{16,0},{24,8},{1,17},{9,25},{17,1},{25,9},{2,18},{10... | collective-permute-start | bytes 786440 | tf_op jit(solution)/shard_map/ppermute | solution.py:24
  66.0 26.6 %collective-permute-start.25 = (bf16[1056,512]{1,0:T(8,128)(2,1)S(1)}, bf16[1056,512]{1,0:T(8,128)(2,1)S(1)}, u32[]{:S(2)}, u32[]{:S(2)}) collective-permute-start(bf16[1056,512]{1,0:T(8,128)(2,1)S(1)} %pad_maximum_fusion.refs_0_), channel_id=1, source_target_pairs={{0,64},{32,96},{64,0},{96,32},{1,65},{33,97},{65,1},{97,33},{2,66}... | collective-permute-start | bytes 3244040 | tf_op jit(solution)/shard_map/ppermute | solution.py:24
  67.5 14.3 %collective-permute-start.20 = (bf16[128,2048]{1,0:T(8,128)(2,1)S(1)}, bf16[128,2048]{1,0:T(8,128)(2,1)S(1)}, u32[]{:S(2)}, u32[]{:S(2)}) collective-permute-start(bf16[128,2048]{1,0:T(8,128)(2,1)S(1)} %get-tuple-element.32.x1), channel_id=1, source_target_pairs={{0,2},{2,4},{4,6},{6,0},{1,3},{3,5},{5,7},{7,1},{8,10},{10,12},{12... | collective-permute-start | bytes 1572872 | tf_op jit(solution)/shard_map/ppermute | solution.py:24
  68.8 28.1 %collective-permute-start.29 = (bf16[1056,512]{1,0:T(8,128)(2,1)S(1)}, bf16[1056,512]{1,0:T(8,128)(2,1)S(1)}, u32[]{:S(2)}, u32[]{:S(2)}) collective-permute-start(bf16[1056,512]{1,0:T(8,128)(2,1)S(1)} %pad_maximum_fusion.refs_0_), channel_id=1, source_target_pairs={{0,1},{1,0},{2,3},{3,2},{4,5},{5,4},{6,7},{7,6},{8,9},{9,8},{10,11... | collective-permute-start | bytes 3244040 | tf_op jit(solution)/shard_map/ppermute | solution.py:24
  69.2 26.8 %collective-permute-start.26 = (bf16[4,1056,128]{2,1,0:T(8,128)(2,1)S(1)}, bf16[4,1056,128]{2,1,0:T(8,128)(2,1)S(1)}, u32[]{:S(2)}, u32[]{:S(2)}) collective-permute-start(bf16[4,1056,128]{2,1,0:T(8,128)(2,1)S(1)} %pad_maximum_fusion.1.refs_1_), channel_id=1, source_target_pairs={{0,16},{8,24},{16,0},{24,8},{1,17},{9,25},{17,1},{25,9},{2,18},{10... | collective-permute-start | bytes 3244040 | tf_op jit(solution)/shard_map/ppermute | solution.py:24
  69.2 48.4 %collective-permute-start.31 = (bf16[1056,512]{1,0:T(8,128)(2,1)S(1)}, bf16[1056,512]{1,0:T(8,128)(2,1)S(1)}, u32[]{:S(2)}, u32[]{:S(2)}) collective-permute-start(bf16[1056,512]{1,0:T(8,128)(2,1)S(1)} %pad_maximum_fusion.refs_0_), channel_id=1, source_target_pairs={{0,96},{32,0},{64,32},{96,64},{1,97},{33,1},{65,33},{97,65},{2,98}... | collective-permute-start | bytes 3244040 | tf_op jit(solution)/shard_map/ppermute | solution.py:24
  81.8 36.5 %collective-permute-start.13 = (bf16[2048,256]{1,0:T(8,128)(2,1)S(1)}, bf16[2048,256]{1,0:T(8,128)(2,1)S(1)}, u32[]{:S(2)}, u32[]{:S(2)}) collective-permute-start(bf16[2048,256]{1,0:T(8,128)(2,1)S(1)} %get-tuple-element.58.in_own), channel_id=1, source_target_pairs={{0,1},{1,0},{2,3},{3,2},{4,5},{5,4},{6,7},{7,6},{8,9},{9,8},{10,11... | collective-permute-start | bytes 3145736 | tf_op jit(solution)/shard_map/ppermute | solution.py:24
  92.6 26.0 %collective-permute-start.18 = (bf16[256,2048]{1,0:T(8,128)(2,1)S(1)}, bf16[256,2048]{1,0:T(8,128)(2,1)S(1)}, u32[]{:S(2)}, u32[]{:S(2)}) collective-permute-start(bf16[256,2048]{1,0:T(8,128)(2,1)S(1)} %get-tuple-element.57.out_own), channel_id=1, source_target_pairs={{0,1},{1,0},{2,3},{3,2},{4,5},{5,4},{6,7},{7,6},{8,9},{9,8},{10,11... | collective-permute-start | bytes 3145736 | tf_op jit(solution)/shard_map/ppermute | solution.py:24
  95.9 32.0 %collective-permute-start.30 = (bf16[4,1056,128]{2,1,0:T(8,128)(2,1)S(1)}, bf16[4,1056,128]{2,1,0:T(8,128)(2,1)S(1)}, u32[]{:S(2)}, u32[]{:S(2)}) collective-permute-start(bf16[4,1056,128]{2,1,0:T(8,128)(2,1)S(1)} %pad_maximum_fusion.1.refs_1_), channel_id=1, source_target_pairs={{0,1},{1,0},{2,3},{3,2},{4,5},{5,4},{6,7},{7,6},{8,9},{9,8},{10,11... | collective-permute-start | bytes 3244040 | tf_op jit(solution)/shard_map/ppermute | solution.py:24
  96.9 32.4 %collective-permute-start.32 = (bf16[4,1056,128]{2,1,0:T(8,128)(2,1)S(1)}, bf16[4,1056,128]{2,1,0:T(8,128)(2,1)S(1)}, u32[]{:S(2)}, u32[]{:S(2)}) collective-permute-start(bf16[4,1056,128]{2,1,0:T(8,128)(2,1)S(1)} %pad_maximum_fusion.1.refs_1_), channel_id=1, source_target_pairs={{0,24},{8,0},{16,8},{24,16},{1,25},{9,1},{17,9},{25,17},{2,26},{10... | collective-permute-start | bytes 3244040 | tf_op jit(solution)/shard_map/ppermute | solution.py:24
  117.6 26.2 %collective-permute-start.35 = (bf16[1056,512]{1,0:T(8,128)(2,1)S(1)}, bf16[1056,512]{1,0:T(8,128)(2,1)S(1)}, u32[]{:S(2)}, u32[]{:S(2)}) collective-permute-start(bf16[1056,512]{1,0:T(8,128)(2,1)S(1)} %pad_maximum_fusion.refs_0_), channel_id=1, source_target_pairs={{0,32},{32,64},{64,96},{96,0},{1,33},{33,65},{65,97},{97,1},{2,34}... | collective-permute-start | bytes 3244040 | tf_op jit(solution)/shard_map/ppermute | solution.py:24
  118.3 28.3 %collective-permute-start.36 = (bf16[4,1056,128]{2,1,0:T(8,128)(2,1)S(1)}, bf16[4,1056,128]{2,1,0:T(8,128)(2,1)S(1)}, u32[]{:S(2)}, u32[]{:S(2)}) collective-permute-start(bf16[4,1056,128]{2,1,0:T(8,128)(2,1)S(1)} %pad_maximum_fusion.1.refs_1_), channel_id=1, source_target_pairs={{0,8},{8,16},{16,24},{24,0},{1,9},{9,17},{17,25},{25,1},{2,10},{10... | collective-permute-start | bytes 3244040 | tf_op jit(solution)/shard_map/ppermute | solution.py:24
  118.5 40.2 %collective-permute-start.33 = (bf16[1056,512]{1,0:T(8,128)(2,1)S(1)}, bf16[1056,512]{1,0:T(8,128)(2,1)S(1)}, u32[]{:S(2)}, u32[]{:S(2)}) collective-permute-start(bf16[1056,512]{1,0:T(8,128)(2,1)S(1)} %collective-permute-done.31.refs_4_), channel_id=1, source_target_pairs={{0,1},{1,0},{2,3},{3,2},{4,5},{5,4},{6,7},{7,6},{8,9},{9,8},{10,11... | collective-permute-start | bytes 3244040 | tf_op jit(solution)/shard_map/ppermute | solution.py:24
  127.9 20.6 %collective-permute-start.21 = (bf16[128,2048]{1,0:T(8,128)(2,1)S(1)}, bf16[128,2048]{1,0:T(8,128)(2,1)S(1)}, u32[]{:S(2)}, u32[]{:S(2)}) collective-permute-start(bf16[128,2048]{1,0:T(8,128)(2,1)S(1)} %get-tuple-element.40), channel_id=1, source_target_pairs={{0,2},{2,4},{4,6},{6,0},{1,3},{3,5},{5,7},{7,1},{8,10},{10,12},{12... | collective-permute-start | bytes 1572872 | tf_op jit(solution)/shard_map/ppermute | solution.py:24
  129.3 25.9 %collective-permute-start.22 = (bf16[128,2048]{1,0:T(8,128)(2,1)S(1)}, bf16[128,2048]{1,0:T(8,128)(2,1)S(1)}, u32[]{:S(2)}, u32[]{:S(2)}) collective-permute-start(bf16[128,2048]{1,0:T(8,128)(2,1)S(1)} %get-tuple-element.41), channel_id=1, source_target_pairs={{0,4},{2,6},{4,0},{6,2},{1,5},{3,7},{5,1},{7,3},{8,12},{10,14},{12... | collective-permute-start | bytes 1572872 | tf_op jit(solution)/shard_map/ppermute | solution.py:24
  143.9 12.4 %collective-permute-start.23 = (bf16[128,2048]{1,0:T(8,128)(2,1)S(1)}, bf16[128,2048]{1,0:T(8,128)(2,1)S(1)}, u32[]{:S(2)}, u32[]{:S(2)}) collective-permute-start(bf16[128,2048]{1,0:T(8,128)(2,1)S(1)} %get-tuple-element.42), channel_id=1, source_target_pairs={{0,6},{2,0},{4,2},{6,4},{1,7},{3,1},{5,3},{7,5},{8,14},{10,8},{12,... | collective-permute-start | bytes 1572872 | tf_op jit(solution)/shard_map/ppermute | solution.py:24
  146.6 12.7 %collective-permute-start.34 = (bf16[4,1056,128]{2,1,0:T(8,128)(2,1)S(1)}, bf16[4,1056,128]{2,1,0:T(8,128)(2,1)S(1)}, u32[]{:S(2)}, u32[]{:S(2)}) collective-permute-start(bf16[4,1056,128]{2,1,0:T(8,128)(2,1)S(1)} %collective-permute-done.32.refs_5_), channel_id=1, source_target_pairs={{0,1},{1,0},{2,3},{3,2},{4,5},{5,4},{6,7},{7,6},{8,9},{9,8},{10,11... | collective-permute-start | bytes 3244040 | tf_op jit(solution)/shard_map/ppermute | solution.py:24
  148.5 13.2 %collective-permute-start.37 = (bf16[1056,512]{1,0:T(8,128)(2,1)S(1)}, bf16[1056,512]{1,0:T(8,128)(2,1)S(1)}, u32[]{:S(2)}, u32[]{:S(2)}) collective-permute-start(bf16[1056,512]{1,0:T(8,128)(2,1)S(1)} %collective-permute-done.35.refs_8_), channel_id=1, source_target_pairs={{0,1},{1,0},{2,3},{3,2},{4,5},{5,4},{6,7},{7,6},{8,9},{9,8},{10,11... | collective-permute-start | bytes 3244040 | tf_op jit(solution)/shard_map/ppermute | solution.py:24
  159.3 14.6 %collective-permute-start.24 = (bf16[128,2048]{1,0:T(8,128)(2,1)S(1)}, bf16[128,2048]{1,0:T(8,128)(2,1)S(1)}, u32[]{:S(2)}, u32[]{:S(2)}) collective-permute-start(bf16[128,2048]{1,0:T(8,128)(2,1)S(1)} %get-tuple-element.45.x1), channel_id=1, source_target_pairs={{0,4},{2,6},{4,0},{6,2},{1,5},{3,7},{5,1},{7,3},{8,12},{10,14},{12... | collective-permute-start | bytes 1572872 | tf_op jit(solution)/shard_map/ppermute | solution.py:24
  161.7 24.4 %collective-permute-start.40 = (bf16[128,2048]{1,0:T(8,128)(2,1)S(1)}, bf16[128,2048]{1,0:T(8,128)(2,1)S(1)}, u32[]{:S(2)}, u32[]{:S(2)}) collective-permute-start(bf16[128,2048]{1,0:T(8,128)(2,1)S(1)} %get-tuple-element.45.x1), channel_id=1, source_target_pairs={{0,6},{2,0},{4,2},{6,4},{1,7},{3,1},{5,3},{7,5},{8,14},{10,8},{12,... | collective-permute-start | bytes 1572872 | tf_op jit(solution)/shard_map/ppermute | solution.py:24
  162.9 23.3 %collective-permute-start.41 = (bf16[128,2048]{1,0:T(8,128)(2,1)S(1)}, bf16[128,2048]{1,0:T(8,128)(2,1)S(1)}, u32[]{:S(2)}, u32[]{:S(2)}) collective-permute-start(bf16[128,2048]{1,0:T(8,128)(2,1)S(1)} %get-tuple-element.45.x1), channel_id=1, source_target_pairs={{0,2},{2,4},{4,6},{6,0},{1,3},{3,5},{5,7},{7,1},{8,10},{10,12},{12... | collective-permute-start | bytes 1572872 | tf_op jit(solution)/shard_map/ppermute | solution.py:24
  193.1 13.7 %collective-permute-start.42 = (bf16[128,2048]{1,0:T(8,128)(2,1)S(1)}, bf16[128,2048]{1,0:T(8,128)(2,1)S(1)}, u32[]{:S(2)}, u32[]{:S(2)}) collective-permute-start(bf16[128,2048]{1,0:T(8,128)(2,1)S(1)} %get-tuple-element.54), channel_id=1, source_target_pairs={{0,2},{2,4},{4,6},{6,0},{1,3},{3,5},{5,7},{7,1},{8,10},{10,12},{12... | collective-permute-start | bytes 1572872 | tf_op jit(solution)/shard_map/ppermute | solution.py:24
  194.0 25.7 %collective-permute-start.43 = (bf16[128,2048]{1,0:T(8,128)(2,1)S(1)}, bf16[128,2048]{1,0:T(8,128)(2,1)S(1)}, u32[]{:S(2)}, u32[]{:S(2)}) collective-permute-start(bf16[128,2048]{1,0:T(8,128)(2,1)S(1)} %get-tuple-element.55), channel_id=1, source_target_pairs={{0,4},{2,6},{4,0},{6,2},{1,5},{3,7},{5,1},{7,3},{8,12},{10,14},{12... | collective-permute-start | bytes 1572872 | tf_op jit(solution)/shard_map/ppermute | solution.py:24
  197.1 22.6 %collective-permute-start.44 = (bf16[128,2048]{1,0:T(8,128)(2,1)S(1)}, bf16[128,2048]{1,0:T(8,128)(2,1)S(1)}, u32[]{:S(2)}, u32[]{:S(2)}) collective-permute-start(bf16[128,2048]{1,0:T(8,128)(2,1)S(1)} %get-tuple-element.56), channel_id=1, source_target_pairs={{0,6},{2,0},{4,2},{6,4},{1,7},{3,1},{5,3},{7,5},{8,14},{10,8},{12,... | collective-permute-start | bytes 1572872 | tf_op jit(solution)/shard_map/ppermute | solution.py:24
  (26 other events, 201.3 us)
